TPU v7x, 128 devices: a whole 4x4x4 slice. The times are simulated.
128 devices in a mesh: sp: 16 (over z, x), fs: 4 (over y), tp: 2 (over core).
Axes of the slice: x: 4, y: 4, z: 4, core: 2. Of those that a mesh axis runs over, the one named last changes fastest.
Arguments:
- tokens: bfloat16 [4, 4096, 2048], P('fs', 'sp', 'tp'), may hold values from -6 to 6
- norm_gain: float32 [2048], replicated, may hold values from 0.1 to 1.9
- query_weight: bfloat16 [2048, 1024], P('fs', 'tp'), may hold values from -1 to 1
- key_weight: bfloat16 [2048, 1024], P('fs', 'tp'), may hold values from -4 to 4
- value_weight: bfloat16 [2048, 1024], P('fs', 'tp'), may hold values from -0.125 to 0.125
- state_query: bfloat16 [2048, 1024], P('fs', 'tp'), may hold values from -0.125 to 0.125
- state_key: bfloat16 [2048, 1024], P('fs', 'tp'), may hold values from -0.125 to 0.125
- state_value: bfloat16 [2048, 1024], P('fs', 'tp'), may hold values from -0.125 to 0.125
- map_lambda: float32 [8], P('tp'), may hold values from 0.3 to 0.8
- diff_gain: float32 [1024], P('tp'), may hold values from 0.1 to 1.9
- decay_rate: float32 [8], P('tp'), may hold values from 0 to 0.04
- state_gain: float32 [1024], P('tp'), may hold values from 0.1 to 1.9
- out_weight: bfloat16 [2048, 2048], replicated, may hold values from -0.125 to 0.125
Outputs:
- mixed: bfloat16 [4, 4096, 2048], P('fs', ('sp', 'tp'))
All inputs are finite; a program needn't handle non-finite values.
Results may differ from a plain program's by a relative error of at most 0.015.
Values may be sent and summed in bfloat16 or wider, within the bound.
A program may use at most 128 MiB of HBM per device.

v0:
```python
import jax
import jax.numpy as jnp
from jax import lax
from jax.sharding import Mesh
from jax.sharding import PartitionSpec as P

DK = 64
DV = 128
DR = 128
SP = ("sp_0", "sp_1")
SP_TP = ("sp_0", "sp_1", "tp")


epsilon = 1e-05
branch_scale = 0.8
masked_score = -1e30


def filled_with(x, identity):
    return jax.tree.map(
        lambda part, zero: jnp.zeros_like(part) + jnp.asarray(zero, part.dtype), x, identity
    )


def carried_in(x, axes, combine, identity):
    before = start = filled_with(x, identity)
    so_far = x
    for axis in reversed(axes):
        size, index = (lax.axis_size(axis), lax.axis_index(axis))
        pieces = jax.tree.map(
            lambda part, kind: lax.all_gather(part.astype(kind), axis),
            so_far,
            (jnp.bfloat16, jnp.bfloat16),
        )
        inside, so_far = (start, start)
        for k in range(size):
            passed = k < index
            so_far = combine(
                so_far, jax.tree.map(lambda part, own: part[k].astype(own.dtype), pieces, x)
            )
            inside = jax.tree.map(lambda new, old: jnp.where(passed, new, old), so_far, inside)
        before = combine(inside, before)
    return before


def from_everyone(x, axis):
    copies = jnp.broadcast_to(x, (lax.axis_size(axis), *x.shape))
    return lax.all_to_all(copies, axis, split_axis=0, concat_axis=0, tiled=True)


def laid_out(tiles, dim):
    lengths = list(tiles.shape[1:])
    lengths[dim] *= tiles.shape[0]
    return jnp.moveaxis(tiles, 0, dim).reshape(lengths)


def gathered_copies(x, axis, dim):
    tiles = from_everyone(x, axis)
    return laid_out(tiles, dim)


def in_one_piece(arrays, axis, dim, along):
    ends, at = ([], 0)
    for a in arrays[:-1]:
        at += a.shape[along]
        ends.append(at)
    both = jnp.concatenate(arrays, axis=along)
    return tuple(jnp.split(lax.all_gather(both, axis, axis=dim, tiled=True), ends, axis=along))


def in_blocks(x, dim, size):
    lengths = x.shape
    tiles = x.reshape(*lengths[:dim], size, lengths[dim] // size, *lengths[dim + 1 :])
    return jnp.moveaxis(tiles, dim, 0)


def sent_and_summed(x, axis, dim):
    size = lax.axis_size(axis)
    tiles = lax.all_to_all(in_blocks(x, dim, size), axis, 0, 0, tiled=True)
    return jnp.sum(tiles.astype(jnp.float32), axis=0)


def attend(att_query, att_keys, att_values, map_lambda, diff_gain):
    tok_rows = att_query.shape[0]
    head_count = map_lambda.shape[0]
    key_width = att_keys.shape[1]
    query_heads = att_query.reshape(tok_rows, head_count, 2, DK)
    sp_index = lax.axis_index(SP)
    query_place = sp_index * tok_rows + jnp.arange(tok_rows)
    own_last = sp_index * tok_rows + tok_rows - 1
    score_scale = DK ** (-0.5)

    def absorb_block(running, inputs):
        key_block, key_place = inputs
        key_heads = key_block[:, :key_width].reshape(tok_rows, head_count, 2, DK)
        value_heads = key_block[:, key_width:].reshape(tok_rows, head_count, DV)
        scores = (
            jnp.einsum(
                "qhmd,khmd->mhqk", query_heads, key_heads, preferred_element_type=jnp.float32
            )
            * score_scale
        )
        causal = key_place[None, :] <= query_place[:, None]
        row_peak, totals, summed = running
        new_peak = jnp.maximum(row_peak, jnp.max(jnp.where(causal, scores, masked_score), axis=-1))
        weights = jnp.where(causal, jnp.exp(scores - new_peak[..., None]), 0.0)
        factor = jnp.exp(row_peak - new_peak)
        totals = totals * factor + jnp.sum(weights, axis=-1)
        summed = summed * factor[..., None] + jnp.einsum(
            "mhqk,khv->mhqv",
            weights.astype(jnp.bfloat16),
            value_heads,
            preferred_element_type=jnp.float32,
        )
        return ((new_peak, totals, summed), None)

    def absorb(running, pieces):
        piece_rows = pieces.shape[0]
        stacked = pieces.reshape(piece_rows // tok_rows, tok_rows, pieces.shape[1])
        places = jnp.arange(piece_rows).reshape(piece_rows // tok_rows, tok_rows)
        return lax.scan(absorb_block, running, (stacked, places))[0]

    starting = (
        jnp.full((2, head_count, tok_rows), masked_score, jnp.float32),
        jnp.zeros((2, head_count, tok_rows), jnp.float32),
        jnp.zeros((2, head_count, tok_rows, DV), jnp.float32),
    )
    joined_kv = jnp.concatenate([att_keys, att_values], axis=1)
    pieces = lax.all_gather(joined_kv, SP, axis=0, tiled=True)
    running = lax.cond(
        jnp.int32(0) <= own_last,
        lambda holding: absorb(holding, pieces),
        lambda holding: holding,
        starting,
    )
    row_peak, totals, summed = running
    averaged = summed / totals[..., None]
    differ = averaged[0] - map_lambda[:, None, None] * averaged[1]
    normed = differ * lax.rsqrt(jnp.mean(differ * differ, axis=-1, keepdims=True) + epsilon)
    normed = normed * diff_gain.reshape(head_count, 1, DV) * branch_scale
    return normed.transpose(1, 0, 2).reshape(tok_rows, head_count * DV).astype(jnp.bfloat16)


def retain(ret_query, ret_keys, ret_values, decay_rate, state_gain):
    tok_rows = ret_query.shape[0]
    head_count = decay_rate.shape[0]
    query_heads = ret_query.reshape(tok_rows, head_count, DR)
    key_heads = ret_keys.reshape(tok_rows, head_count, DR)
    value_heads = ret_values.reshape(tok_rows, head_count, DR)
    position = jnp.arange(tok_rows).astype(jnp.float32)
    distance = position[:, None] - position[None, :]
    decay_col = decay_rate[:, None, None]
    within = jnp.where(distance >= 0, jnp.exp(-decay_col * jnp.maximum(distance, 0.0)), 0.0)
    local_scores = (
        jnp.einsum("qhd,khd->hqk", query_heads, key_heads, preferred_element_type=jnp.float32)
        * within
    )
    intra_out = jnp.einsum(
        "hqk,khv->hqv",
        local_scores.astype(jnp.bfloat16),
        value_heads,
        preferred_element_type=jnp.float32,
    )
    key_decayed = key_heads.astype(jnp.float32) * jnp.exp(
        -decay_rate[None, :, None] * (tok_rows - 1.0 - position)[:, None, None]
    )
    own_state = jnp.einsum("khd,khv->hdv", key_decayed, value_heads.astype(jnp.float32))
    block_decay = jnp.exp(-decay_rate * tok_rows)

    def link_states(earlier, later):
        return (earlier[0] * later[1][:, None, None] + later[0], earlier[1] * later[1])

    identity = (jnp.zeros_like(own_state), jnp.ones_like(block_decay))
    incoming, _ = carried_in((own_state, block_decay), SP, link_states, identity)
    carried = jnp.einsum("qhd,hdv->hqv", query_heads.astype(jnp.float32), incoming)
    carried = carried * jnp.exp(-decay_col * (position + 1.0)[None, :, None])
    combined = intra_out + carried
    normed = combined * lax.rsqrt(jnp.mean(combined * combined, axis=-1, keepdims=True) + epsilon)
    normed = normed * state_gain.reshape(head_count, 1, DR)
    return normed.transpose(1, 0, 2).reshape(tok_rows, head_count * DR).astype(jnp.bfloat16)


def body(
    tokens,
    norm_gain,
    query_weight,
    key_weight,
    value_weight,
    state_query,
    state_key,
    state_value,
    map_lambda,
    diff_gain,
    decay_rate,
    state_gain,
    out_weight,
):
    gathered = gathered_copies(tokens[0], "tp", 1)
    tok_float = gathered.astype(jnp.float32)
    normed = tok_float * lax.rsqrt(
        jnp.mean(tok_float * tok_float, axis=-1, keepdims=True) + epsilon
    )
    normed = (normed * norm_gain).astype(jnp.bfloat16)
    pieces = in_one_piece(
        (query_weight, key_weight, value_weight, state_query, state_key, state_value), "fs", 0, 1
    )
    projected = tuple(
        (jnp.dot(normed, row_block, preferred_element_type=jnp.float32) for row_block in pieces)
    )
    att_query, att_keys, att_values, ret_query, ret_keys, ret_values = (
        member.astype(jnp.bfloat16) for member in projected
    )
    attended = attend(att_query, att_keys, att_values, map_lambda, diff_gain)
    retained = retain(ret_query, ret_keys, ret_values, decay_rate, state_gain)
    joined = jnp.concatenate([attended, retained], axis=1)
    diff_width = attended.shape[1]
    ret_width = retained.shape[1]
    tp_count = lax.axis_size("tp")
    tp_index = lax.axis_index("tp")
    own_rows = jnp.concatenate(
        [
            lax.dynamic_slice_in_dim(out_weight, tp_index * diff_width, diff_width, 0),
            lax.dynamic_slice_in_dim(
                out_weight, tp_count * diff_width + tp_index * ret_width, ret_width, 0
            ),
        ],
        axis=0,
    )
    output = sent_and_summed(
        jnp.dot(joined, own_rows, preferred_element_type=jnp.float32).astype(jnp.bfloat16), "tp", 0
    ).astype(jnp.bfloat16)
    return output[None]


def solution(mesh):
    torus = Mesh(
        mesh.devices.reshape(4, 4, mesh.shape["fs"], mesh.shape["tp"]), ("sp_0", "sp_1", "fs", "tp")
    )
    return jax.shard_map(
        body,
        mesh=torus,
        in_specs=(
            P("fs", SP, "tp"),
            P(),
            P("fs", "tp"),
            P("fs", "tp"),
            P("fs", "tp"),
            P("fs", "tp"),
            P("fs", "tp"),
            P("fs", "tp"),
            P("tp"),
            P("tp"),
            P("tp"),
            P("tp"),
            P(),
        ),
        out_specs=P("fs", SP_TP, None),
        check_vma=False,
    )
```

profile of v0, /device:TPU:65, one launch (start us, length us, event | category | flops | bytes accessed | tf_op | source)
XLA Modules:
  0.0 330.6 jit_solution(11312932430256116211)
XLA Ops:
  13.3 4.9 %all_to_all.10 = bf16[2,256,1024]{1,2,0:T(8,128)(2,1)S(1)} all-to-all(bf16[2,256,1024]{1,2,0:T(8,128)(2,1)S(1)} %broadcast_in_dim.49), channel_id=1, replica_groups=mesh['sp_0'=4,'sp_1'=4,'fs'=4,'tp'=2] {'tp'}, dimensions={0} | all-to-all | bytes 2097152 | tf_op jit(solution)/shard_map/all_to_all | solution.py:48
  18.8 113.2 %all-gather.6.cloned.1.call-done = bf16[2048,3072]{1,0:T(8,128)(2,1)} async-done(((bf16[512,3072]{1,0:T(8,128)(2,1)}), bf16[2048,3072]{1,0:T(8,128)(2,1)}) %all-gather.6.cloned.1.call-update) | async-done | bytes 12582928 | tf_op jit(solution)/shard_map/all_gather | solution.py:68
  132.1 2.3 fusion.36
  134.4 2.3 fusion.33
  139.2 8.4 %all-reduce = bf16[16]{0:T(256)(128)(2,1)S(1)} all-reduce(bf16[16]{0:T(256)(128)(2,1)S(1)} %dynamic-update-slice), channel_id=2, replica_groups=mesh['sp_0'=4,'sp_1'=4,'fs'=4,'tp'=2] {'sp_1'}, use_global_device_ids=true, to_apply=%add | all-reduce | flops 16 | bytes 64
  147.7 6.5 %all-gather.2 = bf16[4,1,4]{2,1,0:T(2,128)(2,1)S(1)} all-gather(bf16[1,1,4]{2,1,0:T(2,128)(2,1)S(1)} %get-tuple-element.136), channel_id=1, replica_groups=mesh['sp_0'=4,'sp_1'=4,'fs'=4,'tp'=2] {'sp_0'}, dimensions={0}, use_global_device_ids=true | all-gather | bytes 40 | tf_op jit(solution)/shard_map/all_gather | solution.py:31
  154.7 4.1 %constant_dynamic-slice_fusion.3 = (bf16[512,2048]{1,0:T(8,128)(2,1)S(1)}, bf16[512,2048]{1,0:T(8,128)(2,1)}) fusion(bf16[2048,2048]{1,0:T(8,128)(2,1)} %param.29, s32[]{:T(128)S(6)} %select_n.134, s32[]{:T(128)S(6)} %select_n.135), kind=kLoop, calls=%fused_computation.191 | loop fusion | bytes 8388616 | tf_op jit(solution)/shard_map/dynamic_slice | solution.py:222
  158.8 3.1 fusion.45
  163.6 2.4 fusion.51
  166.9 12.0 %all-gather.1 = bf16[16,128,128]{2,1,0:T(8,128)(2,1)S(1)} all-gather(bf16[4,128,128]{2,1,0:T(8,128)(2,1)S(1)} %convolution_convert_fusion), channel_id=3, replica_groups=mesh['sp_0'=4,'sp_1'=4,'fs'=4,'tp'=2] {'sp_1'}, dimensions={0}, use_global_device_ids=true | all-gather | bytes 655360 | tf_op jit(solution)/shard_map/all_gather | solution.py:31
  179.1 15.9 %all_gather.33 = bf16[4,4,128,128]{3,2,1,0:T(8,128)(2,1)S(1)} all-gather(bf16[1,4,128,128]{3,2,1,0:T(8,128)(2,1)S(1)} %fusion.90), channel_id=1, replica_groups=mesh['sp_0'=4,'sp_1'=4,'fs'=4,'tp'=2] {'sp_0'}, dimensions={0}, use_global_device_ids=true | all-gather | bytes 655360 | tf_op jit(solution)/shard_map/all_gather | solution.py:31
  195.0 2.3 fusion.54
  199.4 2.7 multiply_reduce_fusion.1
  206.4 6.1 %all-gather.8.cloned.1.call-done = bf16[4096,1024]{1,0:T(8,128)(2,1)} async-done(((bf16[256,1024]{1,0:T(8,128)(2,1)}), bf16[4096,1024]{1,0:T(8,128)(2,1)}) %all-gather.8.cloned.1.call-update) | async-done | bytes 8388624 | tf_op jit(solution)/shard_map/all_gather | solution.py:129
  212.5 100.3 %conditional.1 = (f32[2,4,256]{2,1,0:T(4,128)}, f32[2,4,256,128]{2,3,0,1:T(8,128)}) conditional(s32[]{:T(128)} %convert_element_type.271, () %tuple.17, (bf16[4096,1024]{1,0:T(8,128)(2,1)}, bf16[256,512]{1,0:T(8,128)(2,1)S(1)}, s32[]{:T(128)}, s32[256]{0:T(256)S(1)}) %tuple.18), branch_computations={%region_1.0_spmd, %region_2.7_spmd} | conditional | flops 206391552 | bytes 13727981 | solution.py:130
  212.7 100.1 %while.14 = (s32[]{:T(128)}, f32[2,4,256]{2,1,0:T(4,128)S(1)}, f32[2,4,256]{2,1,0:T(4,128)}, f32[2,4,256,128]{2,3,0,1:T(8,128)}, s32[16,256]{1,0:T(8,128)S(1)}, ...) while((s32[]{:T(128)}, f32[2,4,256]{2,1,0:T(4,128)S(1)}, ...), condition=%wide.region_6.6_spmd.clone, body=%wide.region_3.5_spmd.clone.sunk | while | flops 206383104 | bytes 12660865 | solution.py:121
  221.0 2.5 fusion.177
  227.4 2.5 fusion.177
  233.8 2.5 fusion.177
  240.2 2.5 fusion.177
  246.5 2.5 fusion.177
  252.9 2.5 fusion.177
  259.3 2.5 fusion.177
  265.7 2.5 fusion.177
  272.0 2.5 fusion.177
  278.4 2.5 fusion.177
  284.8 2.5 fusion.177
  291.2 2.5 fusion.177
  297.5 2.5 fusion.177
  303.9 2.5 fusion.177
  310.3 2.5 fusion.177
  316.7 6.0 %all_to_all.11 = bf16[2,128,2048]{2,1,0:T(8,128)(2,1)S(1)} all-to-all(bf16[2,128,2048]{2,1,0:T(8,128)(2,1)S(1)} %bitcast.202), channel_id=1, replica_groups=mesh['sp_0'=4,'sp_1'=4,'fs'=4,'tp'=2] {'tp'}, dimensions={0} | all-to-all | bytes 2097152 | tf_op jit(solution)/shard_map/all_to_all | solution.py:79
  (261 shorter events, 85.6 us)
Async XLA Ops:
  6.5 125.5 %all-gather.6.cloned.1.call-start = ((), (), s32[]{:S(2)}) async-start(), calls=%async_computation.2 | async-start | bytes 15728640 | tf_op jit(solution)/shard_map/all_gather | solution.py:68
  6.5 3.5 %copy-start.2 = (bf16[512,512]{1,0:T(8,128)(2,1)S(1)}, bf16[512,512]{1,0:T(8,128)(2,1)}, u32[]{:S(2)}) copy-start(bf16[512,512]{1,0:T(8,128)(2,1)} %param.22) | copy-start | bytes 1572868
  6.5 3.5 %copy-start.3 = (bf16[512,512]{1,0:T(8,128)(2,1)S(1)}, bf16[512,512]{1,0:T(8,128)(2,1)}, u32[]{:S(2)}) copy-start(bf16[512,512]{1,0:T(8,128)(2,1)} %param.23) | copy-start | bytes 1572868
  6.5 3.6 %copy-start.4 = (bf16[512,512]{1,0:T(8,128)(2,1)S(1)}, bf16[512,512]{1,0:T(8,128)(2,1)}, u32[]{:S(2)}) copy-start(bf16[512,512]{1,0:T(8,128)(2,1)} %param.24) | copy-start | bytes 1572868
  10.2 1.7 copy-start
  11.9 6.6 %copy-start.7 = (f32[2048]{0:T(1024)S(1)}, f32[2048]{0:T(1024)}, u32[]{:S(2)}) copy-start(f32[2048]{0:T(1024)} %param.18) | copy-start | bytes 24580
  11.9 200.6 %all-gather.8.cloned.1.call-start = ((), (), s32[]{:S(2)}) async-start(), calls=%async_computation.3 | async-start | bytes 8912896 | tf_op jit(solution)/shard_map/all_gather | solution.py:129
  134.4 3.3 copy-start.12
  134.4 4.5 %copy-start.11 = (f32[4]{0:T(128)S(1)}, f32[4]{0:T(128)}, u32[]{:S(2)}) copy-start(f32[4]{0:T(128)} %param.27) | copy-start | bytes 52
  163.6 3.1 copy-start.6
  166.0 0.7 copy-start.13
  197.3 0.7 copy-start.14
  197.3 4.7 %copy-start.8 = (f32[512]{0:T(512)S(1)}, f32[512]{0:T(512)}, u32[]{:S(2)}) copy-start(f32[512]{0:T(512)} %param.28) | copy-start | bytes 6148
  212.5 102.5 %copy-start.10 = (f32[4]{0:T(128)S(1)}, f32[4]{0:T(128)}, u32[]{:S(2)}) copy-start(f32[4]{0:T(128)} %param.25) | copy-start | bytes 52
  312.8 2.4 copy-start.9
  312.8 2.6 copy-start.1
  312.8 2.6 copy-start.5
Sparse Core Ops, SparseCore 0:
  12.0 120.0 all-gather.5
  137.8 74.6 all-gather.7
where the time goes:
time: 337 us; the launch traced here: 331 us
  waiting for transfers between devices  119 us (35%)
  matrix products  67.9 us (20%)
  blocking collectives  53.6 us (16%)
  other arithmetic  37.5 us (11%)
  local copies, waits for them, and re-layouts  37.1 us (11%)
  between operations  14.4 us (4%)
    all_gather x1, waiting for transfers between devices, in_one_piece(): lax.all_gather(both, axis, axis=dim, tiled=True)  113 us
    dot_general x16, matrix products, absorb_block(): jnp.einsum('mhqk,khv->mhqv', weights.astype(jnp.bfloat16), value_heads, p...  39.2 us
    all_gather x3, blocking collectives, carried_in(): lax.all_gather(part.astype(kind), axis)  34.4 us
    dynamic_slice x48, local copies, waits for them, and re-layouts, absorb(): return lax.scan(absorb_block, running, (stacked, places))[0]  20.7 us
    add x16, other arithmetic, absorb_block(): totals = totals * factor + jnp.sum(weights, axis=-1)  20.4 us
    dot_general x6, matrix products, body(): jnp.dot(normed, row_block, preferred_element_type=jnp.float32)  14.7 us
    dot_general x16, matrix products, absorb_block(): jnp.einsum('qhmd,khmd->mhqk', query_heads, key_heads, preferred_element_t...  8.6 us
    unnamed x1, blocking collectives  8.38 us
  transfers between devices with their start and end apart: 2, of which 2 were waited for; matrix products, arithmetic and copies ran while one was open for 8% of the time, Pallas kernels for 0%

commit v1 on v0

v1 whole, which is shorter than its diff:
```python
import jax
import jax.numpy as jnp
from jax import lax
from jax.experimental import pallas as pl
from jax.experimental.pallas import tpu as pltpu
from jax.sharding import Mesh
from jax.sharding import PartitionSpec as P

BF16 = jnp.bfloat16
F32 = jnp.float32
MESH = pl.DeviceIdType.MESH
SP = ("sp_0", "sp_1")
SP_TP = ("sp_0", "sp_1", "tp")
FEATURES = 2048
epsilon = 1e-05
branch_scale = 0.8
masked_score = -1e30

DMA = pltpu.SemaphoreType.DMA


def nt_dot(a, b):
    return lax.dot_general(a, b, (((1,), (1,)), ((), ())), preferred_element_type=F32)


def tn_dot(a, b):
    return lax.dot_general(a, b, (((0,), (0,)), ((), ())), preferred_element_type=F32)


def remote(src, dst, send, recv, device):
    return pltpu.make_async_remote_copy(
        src_ref=src, dst_ref=dst, send_sem=send, recv_sem=recv, device_id=device, device_id_type=MESH
    )


def arrival(ref, sem):
    pltpu.make_async_copy(ref, ref, sem).wait()


def kernel(
    tok_hbm, gain, par, wq, wk, wv, sq, sk, sv, ow_hbm, out,
    tok, ss, gl, xs, wa, wb, qkv, kv, qb, ob, join, ow, stat, rs, ps, sin, uu, rb,
    loc, g_s, g_r, w1_s, w1_r, s1_s, s1_r, s1f_s, s1f_r, s2_s, s2_r, s2f_s, s2f_r,
    x_s, x_r, xf_s, xf_r, p_s, p_r, a_s, q_s, kv_r, q_r, f_s, f_r,
    st_s, st_r, pt_s, pt_r, ja_s, jr_s, j_r,
):
    z, x, f, t = (lax.axis_index(a) for a in ("sp_0", "sp_1", "fs", "tp"))
    s = z * 4 + x
    partner = (z, x, f, 1 - t)
    up, down = lax.rem(f + 1, 4), lax.rem(f + 3, 4)

    tok_copy = pltpu.make_async_copy(tok_hbm.at[0], tok, loc.at[0])
    tok_copy.start()
    cols = pl.ds(pl.multiple_of(f * 128, 128), 128)
    own = []
    for g, (w, group) in enumerate(((wa, (wq, wk, wv)), (wb, (sq, sk, sv)))):
        for i, source in enumerate(group):
            c = pltpu.make_async_copy(source.at[:, cols], w.at[0, :, pl.ds(i * 128, 128)], loc.at[1 + g])
            c.start()
    ow_copy = pltpu.make_async_copy(ow_hbm, ow, loc.at[3])
    ow_copy.start()

    srow = pl.ds(pl.multiple_of(s * 32, 32), 32)
    for g, (w, group) in enumerate(((wa, (wq, wk, wv)), (wb, (sq, sk, sv)))):
        for k in range(1, 4):
            fd = lax.rem(f + k, 4)
            for i, source in enumerate(group):
                remote(
                    source.at[srow, pl.ds(pl.multiple_of(fd * 128, 128), 128)],
                    w.at[4 - k, srow, pl.ds(i * 128, 128)],
                    w1_s.at[g], w1_r.at[g], (z, x, fd, t),
                ).start()

    gl_copy = remote(par.at[pl.ds(0, 8), :], gl.at[t], g_s.at[0], g_r.at[0], partner)
    gl_copy.start()
    gl[t] = par[0:8, :]

    tok_copy.wait()

    @pl.loop(0, 8)
    def _(b):
        rows = pl.ds(pl.multiple_of(b * 32, 32), 32)
        v = tok[rows, :].astype(F32)
        v = v * v
        total = v[:, 0:128]
        for k in range(1, 8):
            total = total + v[:, k * 128 : (k + 1) * 128]
        ss[0, rows, :] = total

    ss_copy = remote(ss.at[0], ss.at[1], g_s.at[1], g_r.at[1], partner)
    ss_copy.start()
    ss_copy.wait_recv()

    @pl.loop(0, 8)
    def _(b):
        rows = pl.ds(pl.multiple_of(b * 32, 32), 32)
        total = jnp.sum(ss[0, rows, :] + ss[1, rows, :], axis=-1, keepdims=True)
        r = lax.rsqrt(total * (1.0 / FEATURES) + epsilon)
        v = tok[rows, :].astype(F32) * r * gain[pl.ds(t, 1), :]
        v = v.astype(BF16)
        xs[f, 2 * t, rows, :] = v[:, 0:512]
        xs[f, 2 * t + 1, rows, :] = v[:, 512:1024]

    sends = [gl_copy, ss_copy]

    def xref(e, half):
        return xs.at[lax.rem(f + e, 4), pl.ds(2 * t, 2), pl.ds(half * 128, 128), :]

    def xsend(e, half, target, send, recv):
        c = remote(xref(e, half), xref(e, half), send, recv, (z, x, target, t))
        c.start()
        sends.append(c)

    def xpair(e, half):
        c = remote(xref(e, half), xref(e, half), p_s.at[e, half], p_r.at[e, half], partner)
        c.start()
        sends.append(c)

    xsend(0, 0, up, x_s.at[0, 0], x_r.at[0, 0])
    xsend(0, 1, down, x_s.at[1, 1], x_r.at[1, 1])
    xsend(0, 1, up, x_s.at[0, 1], x_r.at[0, 1])
    xsend(0, 0, down, x_s.at[1, 0], x_r.at[1, 0])
    xpair(0, 0)
    xpair(0, 1)

    ws = (wa, wb)

    def place(g, c1, c2):
        return (c2, c1) if g == 0 else (c1, c2)

    def coords(g):
        return (x, z) if g == 0 else (z, x)

    def share(g, e1, e2, half=None):
        c1, c2 = coords(g)
        pz, px = place(g, lax.rem(c1 + e1, 4), lax.rem(c2 + e2, 4))
        start = (pz * 4 + px) * 32
        if half is None:
            return ws[g].at[pl.ds(1, 3), pl.ds(pl.multiple_of(start, 32), 32), :]
        return ws[g].at[pl.ds(1, 3), pl.ds(pl.multiple_of(start + half * 16, 16), 16), :]

    def wsend(g, ref, d1, d2, send, recv):
        c1, c2 = coords(g)
        pz, px = place(g, lax.rem(c1 + d1, 4), lax.rem(c2 + d2, 4))
        c = remote(ref, ref, send, recv, (pz, px, f, t))
        c.start()
        sends.append(c)

    step = (1, 3)
    origin = (3, 1)

    def second(g, j):
        for d in range(2):
            wsend(g, share(g, j, 0), 0, step[d], s2_s.at[g, j, d], s2_r.at[g, j, d])

    def second_forward(g, j):
        for d in range(2):
            arrival(share(g, j, origin[d]), s2_r.at[g, j, d])
            wsend(g, share(g, j, origin[d], d), 0, step[d], s2f_s.at[g, j, d], s2f_r.at[g, j, d])

    for g in range(2):
        arrival(share(g, 0, 0), w1_r.at[g])
        for d in range(2):
            wsend(g, share(g, 0, 0), step[d], 0, s1_s.at[g, d], s1_r.at[g, d])
        second(g, 0)
    for g in range(2):
        for d in range(2):
            arrival(share(g, origin[d], 0), s1_r.at[g, d])
            wsend(g, share(g, origin[d], 0, d), step[d], 0, s1f_s.at[g, d], s1f_r.at[g, d])
            second(g, origin[d])
    for g in range(2):
        second_forward(g, 0)

    arrival(xref(3, 0), x_r.at[0, 0])
    xsend(3, 0, up, xf_s.at[0], xf_r.at[0])
    xpair(3, 0)
    arrival(xref(1, 1), x_r.at[1, 1])
    xsend(1, 1, down, xf_s.at[1], xf_r.at[1])
    xpair(1, 1)

    for g in range(2):
        for d in range(2):
            arrival(share(g, 2, 0, d), s1f_r.at[g, d])
        second(g, 2)
    for j in (3, 1):
        for g in range(2):
            second_forward(g, j)
    arrival(xref(3, 1), x_r.at[0, 1])
    xpair(3, 1)
    arrival(xref(1, 0), x_r.at[1, 0])
    xpair(1, 0)
    for g in range(2):
        second_forward(g, 2)
    for j in (0, 3, 1, 2):
        for g in range(2):
            for d in range(2):
                arrival(share(g, j, 2, d), s2f_r.at[g, j, d])
    for g in range(2):
        pltpu.make_async_copy(ws[g].at[0], ws[g].at[0], loc.at[1 + g]).wait()

    def arrived_from_partner(e, half):
        q = lax.rem(f + e, 4)
        arrival(xs.at[q, pl.ds(2 * (1 - t), 2), pl.ds(half * 128, 128), :], p_r.at[e, half])

    for e in (0, 3, 1):
        for half in range(2):
            arrived_from_partner(e, half)

    late = jnp.where(s >= 11, 1, 0)

    def att_copies(q):
        found = []
        for c in range(2):
            for h in range(2):
                wanted = (s <= 10) if h == 0 else (s >= 0)
                mine = (q == z) & (2 * t + h == x) & (t == c)
                found.append((
                    remote(qkv.at[q, 1 + c], kv.at[c, s], a_s.at[q, 2 * c + h], kv_r.at[s], (q, 2 * t + h, f, c)),
                    wanted, mine,
                ))
        queries = []
        for c in range(2):
            mine = (q == z) & (2 * t + late == x) & (t == c)
            queries.append((
                remote(
                    qkv.at[q, 0, pl.ds(c * 128, 128), :], qb.at[s], q_s.at[q, c], q_r.at[s],
                    (q, 2 * t + late, f, c),
                ),
                mine,
            ))
        return found, queries

    decay = par[pl.ds(12 + f, 1), :]
    place_rows = lax.broadcasted_iota(jnp.int32, (256, 128), 0).astype(F32)
    key_decay = jnp.exp(-decay * (255.0 - place_rows))

    @pl.loop(0, 4)
    def _(k):
        e = k + (k // 2) * (1 - 2 * lax.rem(k, 2))
        q = lax.rem(f + e, 4)

        @pl.when(k == 3)
        def _():
            for half, up_down in ((0, up), (1, down)):
                arrival(xref(2, half), xf_r.at[half])
                remote(xref(2, half), xref(2, half), p_s.at[2, half], p_r.at[2, half], partner).start()
            for half in range(2):
                arrived_from_partner(2, half)

        for g in range(2):
            total = None
            for d in range(4):
                piece = jnp.dot(xs[q, lax.rem(f + d, 4)], ws[g][d], preferred_element_type=F32)
                total = piece if total is None else total + piece
            total = total.astype(BF16)
            for i in range(3):
                qkv[q, 3 * g + i] = total[:, i * 128 : (i + 1) * 128]

        found, queries = att_copies(q)
        for copy, wanted, mine in found:
            @pl.when(wanted & jnp.logical_not(mine))
            def _():
                copy.start()
        for copy, mine in queries:
            @pl.when(jnp.logical_not(mine))
            def _():
                copy.start()

        @pl.when((q == z) & ((x == 2 * t) & (s <= 10) | (x == 2 * t + 1)))
        def _():
            kv[t, s] = qkv[q, 1 + t]

        @pl.when((q == z) & (x == 2 * t + late))
        def _():
            qb[s] = qkv[q, 0, pl.ds(pl.multiple_of(t * 128, 128), 128), :]

        decayed = (qkv[q, 4].astype(F32) * key_decay).astype(BF16)
        stat[pl.ds(pl.multiple_of(q * 128, 128), 128), :] = tn_dot(decayed, qkv[q, 5]).astype(BF16)

    def st_copy(i):
        return remote(
            stat.at[pl.ds(pl.multiple_of(i * 32, 32), 32), :], rs.at[s], st_s.at[i], st_r.at[s],
            (i // 4, lax.rem(i, 4), f, t),
        )

    def pt_copy(i):
        return remote(
            ps.at[i], sin.at[pl.ds(pl.multiple_of(s * 32, 32), 32), :], pt_s.at[i], pt_r.at[s],
            (i // 4, lax.rem(i, 4), f, t),
        )

    @pl.loop(0, 16)
    def _(i):
        @pl.when(i != s)
        def _():
            st_copy(i).start()

    rs[s] = stat[srow, :]

    decay_square = jnp.broadcast_to(decay[:, 0:1], (256, 256))
    apart = (
        lax.broadcasted_iota(jnp.int32, (256, 256), 0) - lax.broadcasted_iota(jnp.int32, (256, 256), 1)
    ).astype(F32)
    within = jnp.where(apart >= 0, jnp.exp(-decay_square * jnp.maximum(apart, 0.0)), 0.0)

    @pl.loop(0, 4)
    def _(q):
        scores = nt_dot(qkv[q, 3], qkv[q, 4]) * within
        uu[q] = jnp.dot(scores.astype(BF16), qkv[q, 5], preferred_element_type=F32)

    @pl.loop(0, 16)
    def _(i):
        @pl.when(i != s)
        def _():
            arrival(rs.at[i], st_r.at[i])

    block_decay = jnp.exp(-decay * 256.0)
    carry = jnp.zeros((32, 128), F32)
    for i in range(16):
        ps[i] = carry.astype(BF16)
        if i < 15:
            carry = carry * block_decay + rs[i].astype(F32)

    @pl.loop(0, 16)
    def _(i):
        @pl.when(i != s)
        def _():
            pt_copy(i).start()

    sin[srow, :] = ps[s]

    side = lax.rem(x, 2)
    high = x // 2
    head = 4 * high + f
    key_blocks = 11 + 5 * side

    def forward_copy(i):
        return remote(kv.at[t, i], kv.at[t, i], f_s.at[i], f_r.at[i], partner)

    @pl.loop(0, key_blocks)
    def _(i):
        @pl.when(jnp.logical_not((i == s) & (high == t)))
        def _():
            arrival(kv.at[t, i], kv_r.at[i])
        forward_copy(i).start()

    arrival(gl.at[1 - t], g_r.at[0])

    @pl.loop(0, key_blocks)
    def _(i):
        arrival(kv.at[1 - t, i], f_r.at[i])

    lam = gl[high, pl.ds(4 + f, 1), :]
    att_gain = gl[high, pl.ds(f, 1), :] * branch_scale
    lane = lax.broadcasted_iota(jnp.int32, (128, 128), 1)

    def att_out(i):
        return remote(
            ob.at[i], join.at[:, pl.ds(pl.multiple_of(head * 128, 128), 128)], ja_s.at[i], j_r.at[head],
            (i // 4, lax.rem(i, 4), z, t),
        )

    def att_self(i):
        return (i == s) & (z == f)

    first_block = 11 * side

    @pl.loop(first_block, key_blocks)
    def _(i):
        @pl.when(jnp.logical_not((i == s) & (high == t)))
        def _():
            arrival(qb.at[i], q_r.at[i])

        query = qb[i].astype(F32) * 0.125
        stacked = jnp.concatenate(
            [jnp.where(lane < 64, query, 0.0), jnp.where(lane >= 64, query, 0.0)], axis=0
        ).astype(BF16)

        def absorb(j, running, masked):
            peak, total, summed = running
            scores = nt_dot(stacked, kv[0, j])
            if masked:
                row = lax.rem(lax.broadcasted_iota(jnp.int32, (256, 256), 0), 128) + 128 * t
                column = lax.broadcasted_iota(jnp.int32, (256, 256), 1)
                causal = column <= row
                scores = jnp.where(causal, scores, masked_score)
            new_peak = jnp.maximum(peak, jnp.max(scores, axis=-1, keepdims=True))
            weights = jnp.exp(scores - new_peak)
            if masked:
                weights = jnp.where(causal, weights, 0.0)
            factor = jnp.exp(peak - new_peak)
            total = total * factor + jnp.sum(weights, axis=-1, keepdims=True)
            summed = summed * factor + jnp.dot(
                weights.astype(BF16), kv[1, j], preferred_element_type=F32
            )
            return new_peak, total, summed

        running = (
            jnp.full((256, 1), masked_score, F32), jnp.zeros((256, 1), F32), jnp.zeros((256, 128), F32)
        )
        running = lax.fori_loop(0, i, lambda j, r: absorb(j, r, False), running)
        _, total, summed = absorb(i, running, True)
        averaged = summed / total
        differ = averaged[0:128] - lam * averaged[128:256]
        normed = differ * lax.rsqrt(jnp.mean(differ * differ, axis=-1, keepdims=True) + epsilon)
        result = (normed * att_gain).astype(BF16)
        ob[i] = result

        @pl.when(jnp.logical_not(att_self(i)))
        def _():
            att_out(i).start()

        @pl.when(att_self(i))
        def _():
            join[:, pl.ds(pl.multiple_of(head * 128, 128), 128)] = result

    @pl.loop(0, 16)
    def _(i):
        @pl.when(i != s)
        def _():
            arrival(sin.at[pl.ds(pl.multiple_of(i * 32, 32), 32), :], pt_r.at[i])

    ret_head = 8 + 4 * t + f
    ret_cols = pl.ds(pl.multiple_of(ret_head * 128, 128), 128)
    query_decay = jnp.exp(-decay * (place_rows + 1.0))
    state_gain = par[pl.ds(8 + f, 1), :]

    def ret_out(q, c):
        return remote(
            rb.at[q, pl.ds(c * 128, 128), :], join.at[:, ret_cols], jr_s.at[q, c], j_r.at[ret_head], (z, x, q, c)
        )

    def ret_self(q, c):
        return (q == f) & (t == c)

    @pl.loop(0, 4)
    def _(q):
        state = sin[pl.ds(pl.multiple_of(q * 128, 128), 128), :]
        u = uu[q] + jnp.dot(qkv[q, 3], state, preferred_element_type=F32) * query_decay
        normed = u * lax.rsqrt(jnp.mean(u * u, axis=-1, keepdims=True) + epsilon)
        rb[q] = (normed * state_gain).astype(BF16)
        for c in range(2):
            @pl.when(jnp.logical_not(ret_self(q, c)))
            def _():
                ret_out(q, c).start()

            @pl.when(ret_self(q, c))
            def _():
                join[:, ret_cols] = rb[q, c * 128 : (c + 1) * 128, :]

    @pl.loop(0, 8)
    def _(h):
        @pl.when(jnp.logical_not((lax.rem(h, 4) == f) & (z == f) & (x == 2 * (h // 4) + late)))
        def _():
            arrival(ob.at[0], j_r.at[h])

        @pl.when(h != 4 * t + f)
        def _():
            arrival(ob.at[0], j_r.at[8 + h])

    ow_copy.wait()

    @pl.loop(0, 4)
    def _(n):
        span = pl.ds(pl.multiple_of(n * 512, 512), 512)
        out[:, span] = jnp.dot(join[...], ow[:, span], preferred_element_type=F32).astype(BF16)

    for g in range(2):
        arrival(share(g, 0, 0), w1_s.at[g])
    for c in sends:
        c.wait_send()
    for half in range(2):
        remote(xref(2, half), xref(2, half), p_s.at[2, half], p_r.at[2, half], partner).wait_send()

    @pl.loop(0, 4)
    def _(q):
        found, queries = att_copies(q)
        for copy, wanted, mine in found:
            @pl.when(wanted & jnp.logical_not(mine))
            def _():
                copy.wait_send()
        for copy, mine in queries:
            @pl.when(jnp.logical_not(mine))
            def _():
                copy.wait_send()
        for c in range(2):
            @pl.when(jnp.logical_not(ret_self(q, c)))
            def _():
                ret_out(q, c).wait_send()

    @pl.loop(0, 16)
    def _(i):
        @pl.when(i != s)
        def _():
            st_copy(i).wait_send()
            pt_copy(i).wait_send()

    @pl.loop(0, key_blocks)
    def _(i):
        forward_copy(i).wait_send()

    @pl.loop(first_block, key_blocks)
    def _(i):
        @pl.when(jnp.logical_not(att_self(i)))
        def _():
            att_out(i).wait_send()


def body(
    tokens, norm_gain, query_weight, key_weight, value_weight, state_query, state_key, state_value,
    map_lambda, diff_gain, decay_rate, state_gain, out_weight,
):
    wide = lambda v: jnp.broadcast_to(v[:, None], (4, 128))
    params = jnp.concatenate(
        [diff_gain.reshape(4, 128), wide(map_lambda), state_gain.reshape(4, 128), wide(decay_rate)], axis=0
    )
    hbm = pl.BlockSpec(memory_space=pl.ANY)
    vmem = pl.BlockSpec(memory_space=pltpu.VMEM)
    out = pl.pallas_call(
        kernel,
        out_shape=jax.ShapeDtypeStruct((128, FEATURES), BF16),
        in_specs=[hbm, vmem, vmem] + [hbm] * 7,
        out_specs=vmem,
        scratch_shapes=[
            pltpu.VMEM((256, 1024), BF16),
            pltpu.VMEM((2, 256, 128), F32),
            pltpu.VMEM((2, 8, 128), F32),
            pltpu.VMEM((4, 4, 256, 512), BF16),
            pltpu.VMEM((4, 512, 384), BF16),
            pltpu.VMEM((4, 512, 384), BF16),
            pltpu.VMEM((4, 6, 256, 128), BF16),
            pltpu.VMEM((2, 16, 256, 128), BF16),
            pltpu.VMEM((16, 128, 128), BF16),
            pltpu.VMEM((16, 128, 128), BF16),
            pltpu.VMEM((128, FEATURES), BF16),
            pltpu.VMEM((FEATURES, FEATURES), BF16),
            pltpu.VMEM((512, 128), BF16),
            pltpu.VMEM((16, 32, 128), BF16),
            pltpu.VMEM((16, 32, 128), BF16),
            pltpu.VMEM((512, 128), BF16),
            pltpu.VMEM((4, 256, 128), F32),
            pltpu.VMEM((4, 256, 128), BF16),
            DMA((4,)), DMA((2,)), DMA((2,)), DMA((2,)), DMA((2,)),
            DMA((2, 2)), DMA((2, 2)), DMA((2, 2)), DMA((2, 2)),
            DMA((2, 4, 2)), DMA((2, 4, 2)), DMA((2, 4, 2)), DMA((2, 4, 2)),
            DMA((2, 2)), DMA((2, 2)), DMA((2,)), DMA((2,)), DMA((4, 2)), DMA((4, 2)),
            DMA((4, 4)), DMA((4, 2)), DMA((16,)), DMA((16,)), DMA((16,)), DMA((16,)),
            DMA((16,)), DMA((16,)), DMA((16,)), DMA((16,)),
            DMA((16,)), DMA((4, 2)), DMA((16,)),
        ],
        compiler_params=pltpu.CompilerParams(has_side_effects=True, vmem_limit_bytes=60 * 1024 * 1024),
        name="layer",
    )(
        tokens, norm_gain.reshape(2, FEATURES // 2), params,
        query_weight, key_weight, value_weight, state_query, state_key, state_value, out_weight,
    )
    return out[None]


def solution(mesh):
    torus = Mesh(
        mesh.devices.reshape(4, 4, mesh.shape["fs"], mesh.shape["tp"]), ("sp_0", "sp_1", "fs", "tp")
    )
    return jax.shard_map(
        body,
        mesh=torus,
        in_specs=(
            P("fs", SP, "tp"), P(), P("fs", "tp"), P("fs", "tp"), P("fs", "tp"), P("fs", "tp"), P("fs", "tp"),
            P("fs", "tp"), P("tp"), P("tp"), P("tp"), P("tp"), P(),
        ),
        out_specs=P("fs", SP_TP, None),
        check_vma=False,
    )
```

time: 337 us -> 116 us (0.34); the launches traced: 331 us -> 113 us
  waiting for transfers between devices: 119 us -> 0 us
  Pallas kernels: 0 us -> 107 us
  matrix products: 67.9 us -> 0 us
  blocking collectives: 53.6 us -> 0 us
  other arithmetic: 37.5 us -> 1.36 us
  local copies, waits for them, and re-layouts: 37.1 us -> 4.64 us
  between operations: 14.4 us -> 0.01 us
    all_gather x2 -> x0, waiting for transfers between devices: 119 us -> none  [the longest x1 113 us: in_one_piece(): lax.all_gather(both, axis, axis=dim, tiled=True)]
    pallas_call x0 -> x1, Pallas kernels: none -> 107 us  [body(): pl.pallas_call(kernel, out_shape=jax.ShapeDtypeStruct((128, FEATURES), BF...]
    dot_general x42 -> x0, matrix products: 67.9 us -> none  [the longest x16 39.2 us: absorb_block(): jnp.einsum('mhqk,khv->mhqv', weights.astype(jnp.bfloat16), value_heads, p...]
    all_gather x3 -> x0, blocking collectives: 34.4 us -> none  [carried_in(): lax.all_gather(part.astype(kind), axis)]
    dynamic_slice x49 -> x0, local copies, waits for them, and re-layouts: 24.8 us -> none  [the longest x48 20.7 us: absorb(): return lax.scan(absorb_block, running, (stacked, places))[0]]
    add x18 -> x0, other arithmetic: 20.4 us -> none  [the longest x16 20.4 us: absorb_block(): totals = totals * factor + jnp.sum(weights, axis=-1)]
    convert_element_type x23 -> x0, other arithmetic: 11 us -> none  [the longest x16 8.16 us: absorb_block(): weights.astype(jnp.bfloat16)]
    all_to_all x2 -> x0, blocking collectives: 10.9 us -> none  [the longest x1 5.97 us: sent_and_summed(): tiles = lax.all_to_all(in_blocks(x, dim, size), axis, 0, 0, tiled=True)]
  transfers between devices with their start and end apart: 2 -> 0, of which waited for: 2 -> 0; matrix products, arithmetic and copies ran while one was open for 8% -> 0% of each run, Pallas kernels for 0% -> 0%
where the time goes in v1:
time: 116 us; the launch traced here: 113 us
  Pallas kernels  107 us (92%)
  local copies, waits for them, and re-layouts  4.64 us (4%)
  other arithmetic  1.36 us (1%)
    pallas_call x1, Pallas kernels, body(): pl.pallas_call(kernel, out_shape=jax.ShapeDtypeStruct((128, FEATURES), BF...  107 us

profile of v1, /device:TPU:65, one launch (start us, length us, event | category | flops | bytes accessed | tf_op | source)
XLA Modules:
  0.0 113.4 jit_solution(9120157237668947020)
XLA Ops:
  0.0 0.7 pad.1.clone
  0.7 0.7 pad.3.clone
  1.5 1.4 %maximum_maximum_fusion.par = f32[16,128]{1,0:T(8,128)} fusion(f32[4,128]{1,0:T(4,128)} %bitcast.4, f32[4,128]{1,0:T(4,128)} %bitcast.5, f32[16]{0:T(128)S(1)} %pad.3.clone, f32[16]{0:T(128)S(1)} %pad.1.clone), kind=kLoop, calls=%fused_computation | loop fusion | flops 6144 | bytes 12416 | tf_op jit(solution)/shard_map/concatenate | solution.py:514
  2.8 1.3 %reshape.11.gain = f32[2,1024]{1,0:T(2,128)} reshape(f32[2048]{0:T(1024)} %param.14) | data formatting | bytes 16384 | tf_op jit(solution)/shard_map/reshape | solution.py:554
  4.1 107.4 %layer.1 = bf16[128,2048]{1,0:T(8,128)(2,1)} custom-call(bf16[1,256,1024]{2,1,0:T(8,128)(2,1)} %tok_hbm.1, f32[2,1024]{1,0:T(2,128)} %reshape.11.gain, f32[16,128]{1,0:T(8,128)} %maximum_maximum_fusion.par, bf16[512,512]{1,0:T(8,128)(2,1)} %wq.1, bf16[512,512]{1,0:T(8,128)(2,1)} %wk.1, bf16[512,512]{1,0:T(8,128)(2,1)} %wv.1, bf16[512,512]{1,0:T(8,128)(2,1)} %sq.1, ...), custom_call_target="tpu_custom_call" | custom-call | tf_op jit(solution)/shard_map/layer/pallas_call | solution.py:519
  111.6 1.9 %copy.15 = bf16[1,128,2048]{2,1,0:T(8,128)(2,1)} copy(bf16[1,128,2048]{2,1,0:T(8,128)(2,1)} %bitcast.3) | data formatting | bytes 1048576

commit v2 on v1

--- a/solution.py
+++ b/solution.py
@@ -38,8 +38,8 @@
 
 
 def kernel(
-    tok_hbm, gain, par, wq, wk, wv, sq, sk, sv, ow_hbm, out,
-    tok, ss, gl, xs, wa, wb, qkv, kv, qb, ob, join, ow, stat, rs, ps, sin, uu, rb,
+    tok_hbm, norm_gain, diff_gain, state_gain, lambda_hbm, decay_hbm, wq, wk, wv, sq, sk, sv, join,
+    map_lambda, decay_rate, tok, gain, rows, ss, gl, xs, wa, wb, qkv, kk, vv, qb, qs, peaks, sums, ob, stat, rs, ps, sin, uu, rb,
     loc, g_s, g_r, w1_s, w1_r, s1_s, s1_r, s1f_s, s1f_r, s2_s, s2_r, s2f_s, s2f_r,
     x_s, x_r, xf_s, xf_r, p_s, p_r, a_s, q_s, kv_r, q_r, f_s, f_r,
     st_s, st_r, pt_s, pt_r, ja_s, jr_s, j_r,
@@ -48,20 +48,60 @@
     s = z * 4 + x
     partner = (z, x, f, 1 - t)
     up, down = lax.rem(f + 1, 4), lax.rem(f + 3, 4)
+    side = lax.rem(x, 2)
+    high = x // 2
+
+    barrier = pltpu.get_barrier_semaphore()
+    peers = [partner]
+    for k in (1, 3):
+        peers += [(z, lax.rem(x + k, 4), f, t), (lax.rem(z + k, 4), x, f, t)]
+    for k in (1, 2, 3):
+        peers.append((z, x, lax.rem(f + k, 4), t))
+    for peer in peers:
+        pl.semaphore_signal(barrier, inc=1, device_id=peer, device_id_type=MESH)
 
     tok_copy = pltpu.make_async_copy(tok_hbm.at[0], tok, loc.at[0])
     tok_copy.start()
     cols = pl.ds(pl.multiple_of(f * 128, 128), 128)
-    own = []
-    for g, (w, group) in enumerate(((wa, (wq, wk, wv)), (wb, (sq, sk, sv)))):
+    small = [
+        pltpu.make_async_copy(norm_gain.at[pl.ds(pl.multiple_of(t * 1024, 1024), 1024)], gain.at[0], loc.at[3]),
+        pltpu.make_async_copy(diff_gain.at[cols], rows.at[0], loc.at[4]),
+        pltpu.make_async_copy(state_gain.at[cols], rows.at[2], loc.at[5]),
+        pltpu.make_async_copy(lambda_hbm, map_lambda, loc.at[6]),
+        pltpu.make_async_copy(decay_hbm, decay_rate, loc.at[7]),
+    ]
+    for c in small:
+        c.start()
+    groups = tuple(enumerate(((wa, (wq, wk, wv)), (wb, (sq, sk, sv)))))
+    for g, (w, group) in groups:
         for i, source in enumerate(group):
-            c = pltpu.make_async_copy(source.at[:, cols], w.at[0, :, pl.ds(i * 128, 128)], loc.at[1 + g])
-            c.start()
-    ow_copy = pltpu.make_async_copy(ow_hbm, ow, loc.at[3])
-    ow_copy.start()
+            pltpu.make_async_copy(
+                source.at[:, cols], w.at[0, :, pl.ds(i * 128, 128)], loc.at[1 + g]
+            ).start()
+
+    tok_copy.wait()
+
+    @pl.loop(0, 8)
+    def _(b):
+        block = pl.ds(pl.multiple_of(b * 32, 32), 32)
+        v = tok[block, :].astype(F32)
+        v = v * v
+        total = v[:, 0:128]
+        for k in range(1, 8):
+            total = total + v[:, k * 128 : (k + 1) * 128]
+        ss[0, block, :] = total
+
+    for c in small:
+        c.wait()
+    rows[1] = jnp.full((128,), map_lambda[f], F32)
+
+    pl.semaphore_wait(barrier, len(peers))
+
+    ss_copy = remote(ss.at[0], ss.at[1], g_s.at[1], g_r.at[1], partner)
+    ss_copy.start()
 
     srow = pl.ds(pl.multiple_of(s * 32, 32), 32)
-    for g, (w, group) in enumerate(((wa, (wq, wk, wv)), (wb, (sq, sk, sv)))):
+    for g, (w, group) in groups:
         for k in range(1, 4):
             fd = lax.rem(f + k, 4)
             for i, source in enumerate(group):
@@ -71,35 +111,27 @@
                     w1_s.at[g], w1_r.at[g], (z, x, fd, t),
                 ).start()
 
-    gl_copy = remote(par.at[pl.ds(0, 8), :], gl.at[t], g_s.at[0], g_r.at[0], partner)
+    gl_copy = remote(rows, gl.at[t], g_s.at[0], g_r.at[0], partner)
     gl_copy.start()
-    gl[t] = par[0:8, :]
-
-    tok_copy.wait()
+    gl[t] = rows[...]
+    vv[:, :, 128:256] = jnp.ones((16, 256, 128), BF16)
+
+    @pl.when(side == 0)
+    def _():
+        kk[11] = jnp.zeros((256, 128), BF16)
+        vv[11, :, 0:128] = jnp.zeros((256, 128), BF16)
+
+    ss_copy.wait_recv()
 
     @pl.loop(0, 8)
     def _(b):
-        rows = pl.ds(pl.multiple_of(b * 32, 32), 32)
-        v = tok[rows, :].astype(F32)
-        v = v * v
-        total = v[:, 0:128]
-        for k in range(1, 8):
-            total = total + v[:, k * 128 : (k + 1) * 128]
-        ss[0, rows, :] = total
-
-    ss_copy = remote(ss.at[0], ss.at[1], g_s.at[1], g_r.at[1], partner)
-    ss_copy.start()
-    ss_copy.wait_recv()
-
-    @pl.loop(0, 8)
-    def _(b):
-        rows = pl.ds(pl.multiple_of(b * 32, 32), 32)
-        total = jnp.sum(ss[0, rows, :] + ss[1, rows, :], axis=-1, keepdims=True)
+        block = pl.ds(pl.multiple_of(b * 32, 32), 32)
+        total = jnp.sum(ss[0, block, :] + ss[1, block, :], axis=-1, keepdims=True)
         r = lax.rsqrt(total * (1.0 / FEATURES) + epsilon)
-        v = tok[rows, :].astype(F32) * r * gain[pl.ds(t, 1), :]
+        v = tok[block, :].astype(F32) * r * gain[...]
         v = v.astype(BF16)
-        xs[f, 2 * t, rows, :] = v[:, 0:512]
-        xs[f, 2 * t + 1, rows, :] = v[:, 512:1024]
+        xs[f, 2 * t, block, :] = v[:, 0:512]
+        xs[f, 2 * t + 1, block, :] = v[:, 512:1024]
 
     sends = [gl_copy, ss_copy]
 
@@ -208,29 +240,28 @@
 
     late = jnp.where(s >= 11, 1, 0)
 
+    def owner(q, u, c):
+        return (lax.rem(q + u, 4), u, f, c)
+
     def att_copies(q):
+        my_sequence = q == lax.rem(z + 4 - x, 4)
         found = []
+        for h in (1, 0):
+            u = 2 * t + h
+            for c in range(2):
+                target = kk.at[s] if c == 0 else vv.at[s, :, pl.ds(0, 128)]
+                copy = remote(qkv.at[q, 1 + c], target, a_s.at[q, 2 * c + h], kv_r.at[s], owner(q, u, c))
+                elsewhere = jnp.logical_not(my_sequence & (x == u) & (t == c))
+                found.append((copy, elsewhere if h == 1 else elsewhere & (s <= 10)))
+        u = 2 * t + late
         for c in range(2):
-            for h in range(2):
-                wanted = (s <= 10) if h == 0 else (s >= 0)
-                mine = (q == z) & (2 * t + h == x) & (t == c)
-                found.append((
-                    remote(qkv.at[q, 1 + c], kv.at[c, s], a_s.at[q, 2 * c + h], kv_r.at[s], (q, 2 * t + h, f, c)),
-                    wanted, mine,
-                ))
-        queries = []
-        for c in range(2):
-            mine = (q == z) & (2 * t + late == x) & (t == c)
-            queries.append((
-                remote(
-                    qkv.at[q, 0, pl.ds(c * 128, 128), :], qb.at[s], q_s.at[q, c], q_r.at[s],
-                    (q, 2 * t + late, f, c),
-                ),
-                mine,
-            ))
-        return found, queries
-
-    decay = par[pl.ds(12 + f, 1), :]
+            copy = remote(
+                qkv.at[q, 0, pl.ds(c * 128, 128), :], qb.at[s], q_s.at[q, c], q_r.at[s], owner(q, u, c)
+            )
+            found.append((copy, jnp.logical_not(my_sequence & (x == u) & (t == c))))
+        return found
+
+    decay = jnp.full((1, 128), decay_rate[f], F32)
     place_rows = lax.broadcasted_iota(jnp.int32, (256, 128), 0).astype(F32)
     key_decay = jnp.exp(-decay * (255.0 - place_rows))
 
@@ -256,21 +287,24 @@
             for i in range(3):
                 qkv[q, 3 * g + i] = total[:, i * 128 : (i + 1) * 128]
 
-        found, queries = att_copies(q)
-        for copy, wanted, mine in found:
-            @pl.when(wanted & jnp.logical_not(mine))
+        for copy, condition in att_copies(q):
+            @pl.when(condition)
             def _():
                 copy.start()
-        for copy, mine in queries:
-            @pl.when(jnp.logical_not(mine))
-            def _():
-                copy.start()
-
-        @pl.when((q == z) & ((x == 2 * t) & (s <= 10) | (x == 2 * t + 1)))
-        def _():
-            kv[t, s] = qkv[q, 1 + t]
-
-        @pl.when((q == z) & (x == 2 * t + late))
+
+        kept = (q == lax.rem(z + 4 - x, 4)) & (high == t)
+
+        @pl.when(kept & ((side == 1) | (s <= 10)))
+        def _():
+            @pl.when(t == 0)
+            def _():
+                kk[s] = qkv[q, 1]
+
+            @pl.when(t == 1)
+            def _():
+                vv[s, :, 0:128] = qkv[q, 2]
+
+        @pl.when(kept & (side == late))
         def _():
             qb[s] = qkv[q, 0, pl.ds(pl.multiple_of(t * 128, 128), 128), :]
 
@@ -307,6 +341,101 @@
     def _(q):
         scores = nt_dot(qkv[q, 3], qkv[q, 4]) * within
         uu[q] = jnp.dot(scores.astype(BF16), qkv[q, 5], preferred_element_type=F32)
+
+    sequence = lax.rem(z + 4 - x, 4)
+    head = 4 * high + f
+    key_blocks = 11 + 5 * side
+    first_block = 11 * side
+    kv_buffers = (lambda i: kk.at[i], lambda i: vv.at[i, :, pl.ds(0, 128)])
+
+    def forward_copy(c, i):
+        return remote(kv_buffers[c](i), kv_buffers[c](i), f_s.at[i], f_r.at[i], partner)
+
+    for c in range(2):
+        @pl.when(t == c)
+        def _():
+            @pl.loop(0, key_blocks)
+            def _(i):
+                @pl.when(jnp.logical_not((i == s) & (high == t)))
+                def _():
+                    arrival(kv_buffers[c](i), kv_r.at[i])
+                forward_copy(c, i).start()
+
+    arrival(gl.at[1 - t], g_r.at[0])
+
+    @pl.loop(first_block, key_blocks)
+    def _(i):
+        @pl.when(jnp.logical_not((i == s) & (high == t)))
+        def _():
+            arrival(qb.at[i], q_r.at[i])
+
+    @pl.loop(0, key_blocks)
+    def _(i):
+        arrival(qb.at[pl.ds(0, 2)], f_r.at[i])
+
+    lam = gl[high, pl.ds(1, 1), :]
+    att_gain = gl[high, pl.ds(0, 1), :] * branch_scale
+    lane = lax.broadcasted_iota(jnp.int32, (128, 128), 1)
+    join_cols = pl.ds(pl.multiple_of(head * 128, 128), 128)
+
+    def att_out(i):
+        return remote(
+            ob.at[i], join.at[:, join_cols], ja_s.at[i], j_r.at[head], (i // 4, lax.rem(i, 4), sequence, t)
+        )
+
+    def att_self(i):
+        return (i == s) & (sequence == f)
+
+    def attention(first, count, m):
+        for b in range(count):
+            query = qb[first + b].astype(F32) * 0.125
+            qs[b * 256 : b * 256 + 128] = jnp.where(lane < 64, query, 0.0).astype(BF16)
+            qs[b * 256 + 128 : b * 256 + 256] = jnp.where(lane >= 64, query, 0.0).astype(BF16)
+            peaks[b * 256 : b * 256 + 256] = jnp.full((256, 128), masked_score, F32)
+            sums[b * 256 : b * 256 + 256] = jnp.zeros((256, 256), F32)
+
+        def absorb(c, masked):
+            keys = kk[pl.ds(2 * c, 2)].reshape(512, 128)
+            values = vv[pl.ds(2 * c, 2)].reshape(512, 256)
+            for b in range(count):
+                span = slice(b * 256, b * 256 + 256)
+                scores = nt_dot(qs[span], keys)
+                if masked:
+                    row = lax.rem(lax.broadcasted_iota(jnp.int32, (256, 512), 0), 128)
+                    row = row + (128 * t + 256 * (first + b - 2 * m))
+                    column = lax.broadcasted_iota(jnp.int32, (256, 512), 1)
+                    scores = jnp.where(column <= row, scores, masked_score)
+                peak = peaks[span]
+                new_peak = jnp.maximum(peak, jnp.max(scores, axis=-1, keepdims=True))
+                weights = jnp.exp(scores - jnp.concatenate([new_peak] * 4, axis=1)).astype(BF16)
+                factor = jnp.exp(peak - new_peak)
+                sums[span] = sums[span] * jnp.concatenate([factor] * 2, axis=1) + jnp.dot(
+                    weights, values, preferred_element_type=F32
+                )
+                peaks[span] = new_peak
+
+        @pl.loop(0, m)
+        def _(c):
+            absorb(c, False)
+
+        absorb(m, True)
+        for b in range(count):
+            i = first + b
+            averaged = sums[b * 256 : b * 256 + 256, 0:128] / sums[b * 256 : b * 256 + 256, 128:256]
+            differ = averaged[0:128] - lam * averaged[128:256]
+            normed = differ * lax.rsqrt(jnp.mean(differ * differ, axis=-1, keepdims=True) + epsilon)
+            result = (normed * att_gain).astype(BF16)
+            ob[i] = result
+
+            @pl.when(jnp.logical_not(att_self(i)))
+            def _():
+                att_out(i).start()
+
+            @pl.when(att_self(i))
+            def _():
+                join[:, join_cols] = result
+
+    attention(10 + side, 1, 5)
 
     @pl.loop(0, 16)
     def _(i):
@@ -329,90 +458,9 @@
 
     sin[srow, :] = ps[s]
 
-    side = lax.rem(x, 2)
-    high = x // 2
-    head = 4 * high + f
-    key_blocks = 11 + 5 * side
-
-    def forward_copy(i):
-        return remote(kv.at[t, i], kv.at[t, i], f_s.at[i], f_r.at[i], partner)
-
-    @pl.loop(0, key_blocks)
-    def _(i):
-        @pl.when(jnp.logical_not((i == s) & (high == t)))
-        def _():
-            arrival(kv.at[t, i], kv_r.at[i])
-        forward_copy(i).start()
-
-    arrival(gl.at[1 - t], g_r.at[0])
-
-    @pl.loop(0, key_blocks)
-    def _(i):
-        arrival(kv.at[1 - t, i], f_r.at[i])
-
-    lam = gl[high, pl.ds(4 + f, 1), :]
-    att_gain = gl[high, pl.ds(f, 1), :] * branch_scale
-    lane = lax.broadcasted_iota(jnp.int32, (128, 128), 1)
-
-    def att_out(i):
-        return remote(
-            ob.at[i], join.at[:, pl.ds(pl.multiple_of(head * 128, 128), 128)], ja_s.at[i], j_r.at[head],
-            (i // 4, lax.rem(i, 4), z, t),
-        )
-
-    def att_self(i):
-        return (i == s) & (z == f)
-
-    first_block = 11 * side
-
-    @pl.loop(first_block, key_blocks)
-    def _(i):
-        @pl.when(jnp.logical_not((i == s) & (high == t)))
-        def _():
-            arrival(qb.at[i], q_r.at[i])
-
-        query = qb[i].astype(F32) * 0.125
-        stacked = jnp.concatenate(
-            [jnp.where(lane < 64, query, 0.0), jnp.where(lane >= 64, query, 0.0)], axis=0
-        ).astype(BF16)
-
-        def absorb(j, running, masked):
-            peak, total, summed = running
-            scores = nt_dot(stacked, kv[0, j])
-            if masked:
-                row = lax.rem(lax.broadcasted_iota(jnp.int32, (256, 256), 0), 128) + 128 * t
-                column = lax.broadcasted_iota(jnp.int32, (256, 256), 1)
-                causal = column <= row
-                scores = jnp.where(causal, scores, masked_score)
-            new_peak = jnp.maximum(peak, jnp.max(scores, axis=-1, keepdims=True))
-            weights = jnp.exp(scores - new_peak)
-            if masked:
-                weights = jnp.where(causal, weights, 0.0)
-            factor = jnp.exp(peak - new_peak)
-            total = total * factor + jnp.sum(weights, axis=-1, keepdims=True)
-            summed = summed * factor + jnp.dot(
-                weights.astype(BF16), kv[1, j], preferred_element_type=F32
-            )
-            return new_peak, total, summed
-
-        running = (
-            jnp.full((256, 1), masked_score, F32), jnp.zeros((256, 1), F32), jnp.zeros((256, 128), F32)
-        )
-        running = lax.fori_loop(0, i, lambda j, r: absorb(j, r, False), running)
-        _, total, summed = absorb(i, running, True)
-        averaged = summed / total
-        differ = averaged[0:128] - lam * averaged[128:256]
-        normed = differ * lax.rsqrt(jnp.mean(differ * differ, axis=-1, keepdims=True) + epsilon)
-        result = (normed * att_gain).astype(BF16)
-        ob[i] = result
-
-        @pl.when(jnp.logical_not(att_self(i)))
-        def _():
-            att_out(i).start()
-
-        @pl.when(att_self(i))
-        def _():
-            join[:, pl.ds(pl.multiple_of(head * 128, 128), 128)] = result
+    @pl.loop(6 * side, 5 + 3 * side)
+    def _(m):
+        attention(2 * m, 2, m)
 
     @pl.loop(0, 16)
     def _(i):
@@ -423,7 +471,7 @@
     ret_head = 8 + 4 * t + f
     ret_cols = pl.ds(pl.multiple_of(ret_head * 128, 128), 128)
     query_decay = jnp.exp(-decay * (place_rows + 1.0))
-    state_gain = par[pl.ds(8 + f, 1), :]
+    ret_gain = rows[2:3, :]
 
     def ret_out(q, c):
         return remote(
@@ -438,7 +486,7 @@
         state = sin[pl.ds(pl.multiple_of(q * 128, 128), 128), :]
         u = uu[q] + jnp.dot(qkv[q, 3], state, preferred_element_type=F32) * query_decay
         normed = u * lax.rsqrt(jnp.mean(u * u, axis=-1, keepdims=True) + epsilon)
-        rb[q] = (normed * state_gain).astype(BF16)
+        rb[q] = (normed * ret_gain).astype(BF16)
         for c in range(2):
             @pl.when(jnp.logical_not(ret_self(q, c)))
             def _():
@@ -450,20 +498,13 @@
 
     @pl.loop(0, 8)
     def _(h):
-        @pl.when(jnp.logical_not((lax.rem(h, 4) == f) & (z == f) & (x == 2 * (h // 4) + late)))
+        @pl.when(jnp.logical_not((lax.rem(h, 4) == f) & (sequence == f) & (x == 2 * (h // 4) + late)))
         def _():
             arrival(ob.at[0], j_r.at[h])
 
         @pl.when(h != 4 * t + f)
         def _():
             arrival(ob.at[0], j_r.at[8 + h])
-
-    ow_copy.wait()
-
-    @pl.loop(0, 4)
-    def _(n):
-        span = pl.ds(pl.multiple_of(n * 512, 512), 512)
-        out[:, span] = jnp.dot(join[...], ow[:, span], preferred_element_type=F32).astype(BF16)
 
     for g in range(2):
         arrival(share(g, 0, 0), w1_s.at[g])
@@ -474,13 +515,8 @@
 
     @pl.loop(0, 4)
     def _(q):
-        found, queries = att_copies(q)
-        for copy, wanted, mine in found:
-            @pl.when(wanted & jnp.logical_not(mine))
-            def _():
-                copy.wait_send()
-        for copy, mine in queries:
-            @pl.when(jnp.logical_not(mine))
+        for copy, condition in att_copies(q):
+            @pl.when(condition)
             def _():
                 copy.wait_send()
         for c in range(2):
@@ -497,7 +533,7 @@
 
     @pl.loop(0, key_blocks)
     def _(i):
-        forward_copy(i).wait_send()
+        remote(qb.at[pl.ds(0, 2)], qb.at[pl.ds(0, 2)], f_s.at[i], f_r.at[i], partner).wait_send()
 
     @pl.loop(first_block, key_blocks)
     def _(i):
@@ -510,37 +546,39 @@
     tokens, norm_gain, query_weight, key_weight, value_weight, state_query, state_key, state_value,
     map_lambda, diff_gain, decay_rate, state_gain, out_weight,
 ):
-    wide = lambda v: jnp.broadcast_to(v[:, None], (4, 128))
-    params = jnp.concatenate(
-        [diff_gain.reshape(4, 128), wide(map_lambda), state_gain.reshape(4, 128), wide(decay_rate)], axis=0
-    )
-    hbm = pl.BlockSpec(memory_space=pl.ANY)
+    hbm = pl.BlockSpec(memory_space=pltpu.HBM)
     vmem = pl.BlockSpec(memory_space=pltpu.VMEM)
-    out = pl.pallas_call(
+    joined = pl.pallas_call(
         kernel,
         out_shape=jax.ShapeDtypeStruct((128, FEATURES), BF16),
-        in_specs=[hbm, vmem, vmem] + [hbm] * 7,
+        in_specs=[hbm] * 12,
         out_specs=vmem,
         scratch_shapes=[
+            pltpu.SMEM((4,), F32),
+            pltpu.SMEM((4,), F32),
             pltpu.VMEM((256, 1024), BF16),
+            pltpu.VMEM((1, 1024), F32),
+            pltpu.VMEM((8, 128), F32),
             pltpu.VMEM((2, 256, 128), F32),
             pltpu.VMEM((2, 8, 128), F32),
             pltpu.VMEM((4, 4, 256, 512), BF16),
             pltpu.VMEM((4, 512, 384), BF16),
             pltpu.VMEM((4, 512, 384), BF16),
             pltpu.VMEM((4, 6, 256, 128), BF16),
-            pltpu.VMEM((2, 16, 256, 128), BF16),
+            pltpu.VMEM((16, 256, 128), BF16),
+            pltpu.VMEM((16, 256, 256), BF16),
             pltpu.VMEM((16, 128, 128), BF16),
+            pltpu.VMEM((512, 128), BF16),
+            pltpu.VMEM((512, 128), F32),
+            pltpu.VMEM((512, 256), F32),
             pltpu.VMEM((16, 128, 128), BF16),
-            pltpu.VMEM((128, FEATURES), BF16),
-            pltpu.VMEM((FEATURES, FEATURES), BF16),
             pltpu.VMEM((512, 128), BF16),
             pltpu.VMEM((16, 32, 128), BF16),
             pltpu.VMEM((16, 32, 128), BF16),
             pltpu.VMEM((512, 128), BF16),
             pltpu.VMEM((4, 256, 128), F32),
             pltpu.VMEM((4, 256, 128), BF16),
-            DMA((4,)), DMA((2,)), DMA((2,)), DMA((2,)), DMA((2,)),
+            DMA((8,)), DMA((2,)), DMA((2,)), DMA((2,)), DMA((2,)),
             DMA((2, 2)), DMA((2, 2)), DMA((2, 2)), DMA((2, 2)),
             DMA((2, 4, 2)), DMA((2, 4, 2)), DMA((2, 4, 2)), DMA((2, 4, 2)),
             DMA((2, 2)), DMA((2, 2)), DMA((2,)), DMA((2,)), DMA((4, 2)), DMA((4, 2)),
@@ -548,13 +586,21 @@
             DMA((16,)), DMA((16,)), DMA((16,)), DMA((16,)),
             DMA((16,)), DMA((4, 2)), DMA((16,)),
         ],
-        compiler_params=pltpu.CompilerParams(has_side_effects=True, vmem_limit_bytes=60 * 1024 * 1024),
+        compiler_params=pltpu.CompilerParams(
+            collective_id=0, has_side_effects=True, vmem_limit_bytes=32 * 1024 * 1024
+        ),
+        cost_estimate=pl.CostEstimate(flops=40_000_000_000, bytes_accessed=8_000_000, transcendentals=8_000_000),
         name="layer",
     )(
-        tokens, norm_gain.reshape(2, FEATURES // 2), params,
-        query_weight, key_weight, value_weight, state_query, state_key, state_value, out_weight,
+        *(
+            pltpu.with_memory_space_constraint(a, pltpu.HBM)
+            for a in (
+                tokens, norm_gain, diff_gain, state_gain, map_lambda, decay_rate,
+                query_weight, key_weight, value_weight, state_query, state_key, state_value,
+            )
+        )
     )
-    return out[None]
+    return jnp.dot(joined, out_weight, preferred_element_type=F32).astype(BF16)[None]
 
 
 def solution(mesh):

time: 116 us -> 85.6 us (0.74)
  the two profiles are of different devices: /device:TPU:65 before, /device:TPU:1 now
where the time goes in v2:
time: 85.6 us; the launch traced here: 85.5 us
  Pallas kernels  83.5 us (98%)
  matrix products  2.05 us (2%)
    pallas_call x1, Pallas kernels, body(): pl.pallas_call(kernel, out_shape=jax.ShapeDtypeStruct((128, FEATURES), BF...  83.5 us
    dot_general x1, matrix products, body(): jnp.dot(joined, out_weight, preferred_element_type=F32).astype(BF16)[None]  2.05 us

profile of v2, /device:TPU:1, one launch (start us, length us, event | category | flops | bytes accessed | tf_op | source)
XLA Modules:
  0.0 85.5 jit_solution(5382133668459309844)
XLA Ops:
  0.0 0.0 copy-start
  0.0 83.5 %layer.1 = bf16[128,2048]{1,0:T(8,128)(2,1)S(1)} custom-call(bf16[1,256,1024]{2,1,0:T(8,128)(2,1)} %tok_hbm.1, f32[2048]{0:T(1024)} %norm_gain.1, f32[512]{0:T(512)} %diff_gain.1, f32[512]{0:T(512)} %state_gain.1, f32[4]{0:T(128)} %lambda_hbm.1, f32[4]{0:T(128)} %decay_hbm.1, bf16[512,512]{1,0:T(8,128)(2,1)} %wq.1, bf16[512,512]{1,0:T(8,128)(2,1)} %wk.1, ...), custom_call_target="tpu_custom_call" | custom-call | flops 40000000000 | bytes 8000000 | tf_op jit(solution)/shard_map/layer/pallas_call | solution.py:551
  83.5 0.0 copy-done
  83.5 2.1 %fusion = bf16[1,128,2048]{2,1,0:T(8,128)(2,1)} fusion(bf16[128,2048]{1,0:T(8,128)(2,1)S(1)} %layer.1, bf16[2048,2048]{1,0:T(8,128)(2,1)S(1)} %copy-done), kind=kOutput, calls=%fused_computation.1 | convolution fusion | flops 1074003968 | bytes 9437184 | tf_op jit(solution)/shard_map/dot_general | solution.py:603
Async XLA Ops:
  0.0 83.5 %copy-start = (bf16[2048,2048]{1,0:T(8,128)(2,1)S(1)}, bf16[2048,2048]{1,0:T(8,128)(2,1)}, u32[]{:S(2)}) copy-start(bf16[2048,2048]{1,0:T(8,128)(2,1)} %param.25) | copy-start | bytes 25165828

commit v3 on v2

--- a/solution.py
+++ b/solution.py
@@ -39,7 +39,7 @@
 
 def kernel(
     tok_hbm, norm_gain, diff_gain, state_gain, lambda_hbm, decay_hbm, wq, wk, wv, sq, sk, sv, join,
-    map_lambda, decay_rate, tok, gain, rows, ss, gl, xs, wa, wb, qkv, kk, vv, qb, qs, peaks, sums, ob, stat, rs, ps, sin, uu, rb,
+    map_lambda, decay_rate, tok, gain, rows, ss, gl, xs, ws, qkv, kk, vv, qb, qs, sums, ob, stat, rs, ps, sin, uu, rb,
     loc, g_s, g_r, w1_s, w1_r, s1_s, s1_r, s1f_s, s1f_r, s2_s, s2_r, s2f_s, s2f_r,
     x_s, x_r, xf_s, xf_r, p_s, p_r, a_s, q_s, kv_r, q_r, f_s, f_r,
     st_s, st_r, pt_s, pt_r, ja_s, jr_s, j_r,
@@ -72,11 +72,11 @@
     ]
     for c in small:
         c.start()
-    groups = tuple(enumerate(((wa, (wq, wk, wv)), (wb, (sq, sk, sv)))))
-    for g, (w, group) in groups:
+    groups = tuple(enumerate(((wq, wk, wv), (sq, sk, sv))))
+    for g, group in groups:
         for i, source in enumerate(group):
             pltpu.make_async_copy(
-                source.at[:, cols], w.at[0, :, pl.ds(i * 128, 128)], loc.at[1 + g]
+                source.at[:, cols], ws.at[0, :, pl.ds((3 * g + i) * 128, 128)], loc.at[1 + g]
             ).start()
 
     tok_copy.wait()
@@ -101,13 +101,13 @@
     ss_copy.start()
 
     srow = pl.ds(pl.multiple_of(s * 32, 32), 32)
-    for g, (w, group) in groups:
+    for g, group in groups:
         for k in range(1, 4):
             fd = lax.rem(f + k, 4)
             for i, source in enumerate(group):
                 remote(
                     source.at[srow, pl.ds(pl.multiple_of(fd * 128, 128), 128)],
-                    w.at[4 - k, srow, pl.ds(i * 128, 128)],
+                    ws.at[4 - k, srow, pl.ds((3 * g + i) * 128, 128)],
                     w1_s.at[g], w1_r.at[g], (z, x, fd, t),
                 ).start()
 
@@ -155,8 +155,6 @@
     xpair(0, 0)
     xpair(0, 1)
 
-    ws = (wa, wb)
-
     def place(g, c1, c2):
         return (c2, c1) if g == 0 else (c1, c2)
 
@@ -168,8 +166,8 @@
         pz, px = place(g, lax.rem(c1 + e1, 4), lax.rem(c2 + e2, 4))
         start = (pz * 4 + px) * 32
         if half is None:
-            return ws[g].at[pl.ds(1, 3), pl.ds(pl.multiple_of(start, 32), 32), :]
-        return ws[g].at[pl.ds(1, 3), pl.ds(pl.multiple_of(start + half * 16, 16), 16), :]
+            return ws.at[pl.ds(1, 3), pl.ds(pl.multiple_of(start, 32), 32), pl.ds(g * 384, 384)]
+        return ws.at[pl.ds(1, 3), pl.ds(pl.multiple_of(start + half * 16, 16), 16), pl.ds(g * 384, 384)]
 
     def wsend(g, ref, d1, d2, send, recv):
         c1, c2 = coords(g)
@@ -228,13 +226,16 @@
             for d in range(2):
                 arrival(share(g, j, 2, d), s2f_r.at[g, j, d])
     for g in range(2):
-        pltpu.make_async_copy(ws[g].at[0], ws[g].at[0], loc.at[1 + g]).wait()
+        arrival(ws.at[0, :, pl.ds(g * 384, 384)], loc.at[1 + g])
 
     def arrived_from_partner(e, half):
         q = lax.rem(f + e, 4)
         arrival(xs.at[q, pl.ds(2 * (1 - t), 2), pl.ds(half * 128, 128), :], p_r.at[e, half])
 
-    for e in (0, 3, 1):
+    for half, target in ((0, up), (1, down)):
+        arrival(xref(2, half), xf_r.at[half])
+        xpair(2, half)
+    for e in range(4):
         for half in range(2):
             arrived_from_partner(e, half)
 
@@ -267,25 +268,11 @@
 
     @pl.loop(0, 4)
     def _(k):
-        e = k + (k // 2) * (1 - 2 * lax.rem(k, 2))
-        q = lax.rem(f + e, 4)
-
-        @pl.when(k == 3)
-        def _():
-            for half, up_down in ((0, up), (1, down)):
-                arrival(xref(2, half), xf_r.at[half])
-                remote(xref(2, half), xref(2, half), p_s.at[2, half], p_r.at[2, half], partner).start()
-            for half in range(2):
-                arrived_from_partner(2, half)
-
-        for g in range(2):
-            total = None
-            for d in range(4):
-                piece = jnp.dot(xs[q, lax.rem(f + d, 4)], ws[g][d], preferred_element_type=F32)
-                total = piece if total is None else total + piece
-            total = total.astype(BF16)
-            for i in range(3):
-                qkv[q, 3 * g + i] = total[:, i * 128 : (i + 1) * 128]
+        q = lax.rem(z + x + k, 4)
+        features = jnp.concatenate([xs[q, lax.rem(f + d, 4)] for d in range(4)], axis=1)
+        total = jnp.dot(features, ws[...].reshape(FEATURES, 768), preferred_element_type=F32).astype(BF16)
+        for i in range(6):
+            qkv[q, i] = total[:, i * 128 : (i + 1) * 128]
 
         for copy, condition in att_copies(q):
             @pl.when(condition)
@@ -386,39 +373,23 @@
     def att_self(i):
         return (i == s) & (sequence == f)
 
-    def attention(first, count, m):
+    def attention(first, count, m, height):
         for b in range(count):
             query = qb[first + b].astype(F32) * 0.125
             qs[b * 256 : b * 256 + 128] = jnp.where(lane < 64, query, 0.0).astype(BF16)
             qs[b * 256 + 128 : b * 256 + 256] = jnp.where(lane >= 64, query, 0.0).astype(BF16)
-            peaks[b * 256 : b * 256 + 256] = jnp.full((256, 128), masked_score, F32)
-            sums[b * 256 : b * 256 + 256] = jnp.zeros((256, 256), F32)
-
-        def absorb(c, masked):
-            keys = kk[pl.ds(2 * c, 2)].reshape(512, 128)
-            values = vv[pl.ds(2 * c, 2)].reshape(512, 256)
-            for b in range(count):
-                span = slice(b * 256, b * 256 + 256)
-                scores = nt_dot(qs[span], keys)
-                if masked:
-                    row = lax.rem(lax.broadcasted_iota(jnp.int32, (256, 512), 0), 128)
-                    row = row + (128 * t + 256 * (first + b - 2 * m))
-                    column = lax.broadcasted_iota(jnp.int32, (256, 512), 1)
-                    scores = jnp.where(column <= row, scores, masked_score)
-                peak = peaks[span]
-                new_peak = jnp.maximum(peak, jnp.max(scores, axis=-1, keepdims=True))
-                weights = jnp.exp(scores - jnp.concatenate([new_peak] * 4, axis=1)).astype(BF16)
-                factor = jnp.exp(peak - new_peak)
-                sums[span] = sums[span] * jnp.concatenate([factor] * 2, axis=1) + jnp.dot(
-                    weights, values, preferred_element_type=F32
-                )
-                peaks[span] = new_peak
-
-        @pl.loop(0, m)
-        def _(c):
-            absorb(c, False)
-
-        absorb(m, True)
+        keys = kk[0 : 2 * m + 2].reshape(512 * m + 512, 128)
+        values = vv[0 : 2 * m + 2].reshape(512 * m + 512, 256)
+        for b in range(256 * count // height):
+            span = slice(b * height, b * height + height)
+            scores = nt_dot(qs[span], keys)
+            row = lax.broadcasted_iota(jnp.int32, (height, 512), 0) + b * height
+            row = lax.rem(row, 128) + 256 * (row // 256) + (128 * t + 256 * (first - 2 * m))
+            column = lax.broadcasted_iota(jnp.int32, (height, 512), 1)
+            last = jnp.where(column <= row, scores[:, 512 * m :], masked_score)
+            scores = jnp.concatenate([scores[:, : 512 * m], last], axis=1) if m else last
+            weights = jnp.exp(scores - jnp.max(scores, axis=-1, keepdims=True))
+            sums[span] = jnp.dot(weights.astype(BF16), values, preferred_element_type=F32)
         for b in range(count):
             i = first + b
             averaged = sums[b * 256 : b * 256 + 256, 0:128] / sums[b * 256 : b * 256 + 256, 128:256]
@@ -435,7 +406,7 @@
             def _():
                 join[:, join_cols] = result
 
-    attention(10 + side, 1, 5)
+    attention(10 + side, 1, 5, 128)
 
     @pl.loop(0, 16)
     def _(i):
@@ -458,9 +429,15 @@
 
     sin[srow, :] = ps[s]
 
-    @pl.loop(6 * side, 5 + 3 * side)
-    def _(m):
-        attention(2 * m, 2, m)
+    @pl.when(side == 0)
+    def _():
+        for m in range(5):
+            attention(2 * m, 2, m, 256)
+
+    @pl.when(side == 1)
+    def _():
+        for m in (6, 7):
+            attention(2 * m, 2, m, 256)
 
     @pl.loop(0, 16)
     def _(i):
@@ -510,8 +487,6 @@
         arrival(share(g, 0, 0), w1_s.at[g])
     for c in sends:
         c.wait_send()
-    for half in range(2):
-        remote(xref(2, half), xref(2, half), p_s.at[2, half], p_r.at[2, half], partner).wait_send()
 
     @pl.loop(0, 4)
     def _(q):
@@ -562,14 +537,12 @@
             pltpu.VMEM((2, 256, 128), F32),
             pltpu.VMEM((2, 8, 128), F32),
             pltpu.VMEM((4, 4, 256, 512), BF16),
-            pltpu.VMEM((4, 512, 384), BF16),
-            pltpu.VMEM((4, 512, 384), BF16),
+            pltpu.VMEM((4, 512, 768), BF16),
             pltpu.VMEM((4, 6, 256, 128), BF16),
             pltpu.VMEM((16, 256, 128), BF16),
             pltpu.VMEM((16, 256, 256), BF16),
             pltpu.VMEM((16, 128, 128), BF16),
             pltpu.VMEM((512, 128), BF16),
-            pltpu.VMEM((512, 128), F32),
             pltpu.VMEM((512, 256), F32),
             pltpu.VMEM((16, 128, 128), BF16),
             pltpu.VMEM((512, 128), BF16),

time: 85.6 us -> 75.9 us (0.89)
  the two profiles are of different devices: /device:TPU:1 before, /device:TPU:55 now
where the time goes in v3:
time: 75.9 us; the launch traced here: 75.8 us
  Pallas kernels  73.7 us (97%)
  matrix products  2.06 us (3%)
    pallas_call x1, Pallas kernels, body(): pl.pallas_call(kernel, out_shape=jax.ShapeDtypeStruct((128, FEATURES), BF...  73.7 us
    dot_general x1, matrix products, body(): jnp.dot(joined, out_weight, preferred_element_type=F32).astype(BF16)[None]  2.06 us

profile of v3, /device:TPU:55, one launch (start us, length us, event | category | flops | bytes accessed | tf_op | source)
XLA Modules:
  0.0 75.8 jit_solution(14864094392758096331)
XLA Ops:
  0.0 0.0 copy-start
  0.0 73.7 %layer.1 = bf16[128,2048]{1,0:T(8,128)(2,1)S(1)} custom-call(bf16[1,256,1024]{2,1,0:T(8,128)(2,1)} %tok_hbm.1, f32[2048]{0:T(1024)} %norm_gain.1, f32[512]{0:T(512)} %diff_gain.1, f32[512]{0:T(512)} %state_gain.1, f32[4]{0:T(128)} %lambda_hbm.1, f32[4]{0:T(128)} %decay_hbm.1, bf16[512,512]{1,0:T(8,128)(2,1)} %wq.1, bf16[512,512]{1,0:T(8,128)(2,1)} %wk.1, ...), custom_call_target="tpu_custom_call" | custom-call | flops 40000000000 | bytes 8000000 | tf_op jit(solution)/shard_map/layer/pallas_call | solution.py:526
  73.7 0.0 copy-done
  73.7 2.1 %fusion = bf16[1,128,2048]{2,1,0:T(8,128)(2,1)} fusion(bf16[128,2048]{1,0:T(8,128)(2,1)S(1)} %layer.1, bf16[2048,2048]{1,0:T(8,128)(2,1)S(1)} %copy-done), kind=kOutput, calls=%fused_computation.1 | convolution fusion | flops 1074003968 | bytes 9437184 | tf_op jit(solution)/shard_map/dot_general | solution.py:576
Async XLA Ops:
  0.0 73.7 %copy-start = (bf16[2048,2048]{1,0:T(8,128)(2,1)S(1)}, bf16[2048,2048]{1,0:T(8,128)(2,1)}, u32[]{:S(2)}) copy-start(bf16[2048,2048]{1,0:T(8,128)(2,1)} %param.25) | copy-start | bytes 25165828

commit v4 on v3

v4 whole, which is shorter than its diff:
```python
import jax
import jax.numpy as jnp
from jax import lax
from jax.experimental import pallas as pl
from jax.experimental.pallas import tpu as pltpu
from jax.sharding import Mesh
from jax.sharding import PartitionSpec as P

BF16 = jnp.bfloat16
F32 = jnp.float32
MESH = pl.DeviceIdType.MESH
SP = ("sp_0", "sp_1")
SP_TP = ("sp_0", "sp_1", "tp")
FEATURES = 2048
epsilon = 1e-05
branch_scale = 0.8
masked_score = -1e30

DMA = pltpu.SemaphoreType.DMA


def nt_dot(a, b):
    return lax.dot_general(a, b, (((1,), (1,)), ((), ())), preferred_element_type=F32)


def tn_dot(a, b):
    return lax.dot_general(a, b, (((0,), (0,)), ((), ())), preferred_element_type=F32)


def remote(src, dst, send, recv, device):
    return pltpu.make_async_remote_copy(
        src_ref=src, dst_ref=dst, send_sem=send, recv_sem=recv, device_id=device, device_id_type=MESH
    )


def arrival(ref, sem):
    pltpu.make_async_copy(ref, ref, sem).wait()


def kernel(
    tok_hbm, norm_gain, diff_gain, state_gain, lambda_hbm, decay_hbm, wq, wk, wv, sq, sk, sv, ow_hbm, out_hbm,
    map_lambda, decay_rate, tok, gain, rows, ss, gl, xs, ws, stage, qkv, kk, vv, qb, qs, sums, ob, join, ow, summed, rounded, stat, rs, ps, sin, uu, rb,
    loc, once, w1_r, s1_r, s1f_r, s2_r, x_r, xf_r, kv_r, j_r,
):
    (
        ss_s, ss_r, gl_s, gl_r, w1_s, w_s, x_s, p_s, a_s, q_s, f_s, st_s, pt_s, ja_s, jr_s,
        q_r, f_r, st_r, pt_r, jr_r, s2f_r, p_r, p2_r,
    ) = (once.at[i] for i in range(23))
    z, x, f, t = (lax.axis_index(a) for a in ("sp_0", "sp_1", "fs", "tp"))
    s = z * 4 + x
    partner = (z, x, f, 1 - t)
    up, down = lax.rem(f + 1, 4), lax.rem(f + 3, 4)
    side = lax.rem(z, 2)
    high = x // 2

    barrier = pltpu.get_barrier_semaphore()
    peers = [partner]
    for k in (1, 3):
        peers += [(z, lax.rem(x + k, 4), f, t), (lax.rem(z + k, 4), x, f, t)]
    for k in (1, 2, 3):
        peers.append((z, x, lax.rem(f + k, 4), t))
    for peer in peers:
        pl.semaphore_signal(barrier, inc=1, device_id=peer, device_id_type=MESH)

    tok_copy = pltpu.make_async_copy(tok_hbm.at[0], tok, loc.at[0])
    tok_copy.start()
    cols = pl.ds(pl.multiple_of(f * 128, 128), 128)
    small = [
        pltpu.make_async_copy(norm_gain.at[pl.ds(pl.multiple_of(t * 1024, 1024), 1024)], gain.at[0], loc.at[3]),
        pltpu.make_async_copy(diff_gain.at[cols], rows.at[0], loc.at[4]),
        pltpu.make_async_copy(state_gain.at[cols], rows.at[2], loc.at[5]),
        pltpu.make_async_copy(lambda_hbm, map_lambda, loc.at[6]),
        pltpu.make_async_copy(decay_hbm, decay_rate, loc.at[7]),
    ]
    for c in small:
        c.start()
    groups = tuple(enumerate(((wq, wk, wv), (sq, sk, sv))))
    srow = pl.ds(pl.multiple_of(s * 32, 32), 32)
    for g, group in groups:
        for k in range(1, 4):
            theirs = pl.ds(pl.multiple_of(lax.rem(f + k, 4) * 128, 128), 128)
            for i, source in enumerate(group):
                pltpu.make_async_copy(
                    source.at[srow, theirs], stage.at[k - 1, :, pl.ds((3 * g + i) * 128, 128)], loc.at[8 + g]
                ).start()
    for g, group in groups:
        for i, source in enumerate(group):
            pltpu.make_async_copy(
                source.at[:, cols], ws.at[0, :, pl.ds((3 * g + i) * 128, 128)], loc.at[1 + g]
            ).start()

    ow_copy = pltpu.make_async_copy(ow_hbm, ow, loc.at[10])
    ow_copy.start()

    tok_copy.wait()

    @pl.loop(0, 8)
    def _(b):
        block = pl.ds(pl.multiple_of(b * 32, 32), 32)
        v = tok[block, :].astype(F32)
        v = v * v
        total = v[:, 0:128]
        for k in range(1, 8):
            total = total + v[:, k * 128 : (k + 1) * 128]
        ss[0, block, :] = total

    for c in small:
        c.wait()
    rows[1] = jnp.full((128,), map_lambda[f], F32)

    pl.semaphore_wait(barrier, len(peers))

    ss_copy = remote(ss.at[0], ss.at[1], ss_s, ss_r, partner)
    ss_copy.start()

    for g in range(2):
        part = pl.ds(g * 384, 384)
        arrival(stage.at[:, :, part], loc.at[8 + g])
        for k in range(1, 4):
            c = remote(
                stage.at[k - 1, :, part], ws.at[4 - k, srow, part], w1_s, w1_r.at[g],
                (z, x, lax.rem(f + k, 4), t),
            )
            c.start()

    gl_copy = remote(rows, gl.at[t], gl_s, gl_r, partner)
    gl_copy.start()
    gl[t] = rows[...]

    ss_copy.wait_recv()

    @pl.loop(0, 8)
    def _(b):
        block = pl.ds(pl.multiple_of(b * 32, 32), 32)
        total = jnp.sum(ss[0, block, :] + ss[1, block, :], axis=-1, keepdims=True)
        r = lax.rsqrt(total * (1.0 / FEATURES) + epsilon)
        v = tok[block, :].astype(F32) * r * gain[...]
        v = v.astype(BF16)
        xs[f, 2 * t, block, :] = v[:, 0:512]
        xs[f, 2 * t + 1, block, :] = v[:, 512:1024]


    def xref(e, half):
        return xs.at[lax.rem(f + e, 4), pl.ds(2 * t, 2), pl.ds(half * 128, 128), :]

    def xsend(e, half, target, recv):
        remote(xref(e, half), xref(e, half), x_s, recv, (z, x, target, t)).start()

    def xpair(e, half):
        remote(xref(e, half), xref(e, half), p_s, p2_r if e == 2 else p_r, partner).start()

    xsend(0, 0, up, x_r.at[0, 0])
    xsend(0, 1, down, x_r.at[1, 1])
    xsend(0, 1, up, x_r.at[0, 1])
    xsend(0, 0, down, x_r.at[1, 0])
    xpair(0, 0)
    xpair(0, 1)

    vv[:, :, 128:256] = jnp.ones((16, 256, 128), BF16)

    @pl.when(side == 0)
    def _():
        kk[11] = jnp.zeros((256, 128), BF16)
        vv[11, :, 0:128] = jnp.zeros((256, 128), BF16)

    def place(g, c1, c2):
        return (c2, c1) if g == 0 else (c1, c2)

    def coords(g):
        return (x, z) if g == 0 else (z, x)

    def share(g, e1, e2, half=None):
        c1, c2 = coords(g)
        pz, px = place(g, lax.rem(c1 + e1, 4), lax.rem(c2 + e2, 4))
        start = (pz * 4 + px) * 32
        if half is None:
            return ws.at[pl.ds(1, 3), pl.ds(pl.multiple_of(start, 32), 32), pl.ds(g * 384, 384)]
        return ws.at[pl.ds(1, 3), pl.ds(pl.multiple_of(start + half * 16, 16), 16), pl.ds(g * 384, 384)]

    def wsend(g, ref, d1, d2, recv):
        c1, c2 = coords(g)
        pz, px = place(g, lax.rem(c1 + d1, 4), lax.rem(c2 + d2, 4))
        remote(ref, ref, w_s, recv, (pz, px, f, t)).start()

    step = (1, 3)
    origin = (3, 1)

    def second(g, j):
        for d in range(2):
            wsend(g, share(g, j, 0), 0, step[d], s2_r.at[g, j, d])

    def second_forward(g, j):
        for d in range(2):
            arrival(share(g, j, origin[d]), s2_r.at[g, j, d])
            wsend(g, share(g, j, origin[d], d), 0, step[d], s2f_r)

    for g in range(2):
        arrival(share(g, 0, 0), w1_r.at[g])
        for d in range(2):
            wsend(g, share(g, 0, 0), step[d], 0, s1_r.at[g, d])
        second(g, 0)
    for g in range(2):
        for d in range(2):
            arrival(share(g, origin[d], 0), s1_r.at[g, d])
            wsend(g, share(g, origin[d], 0, d), step[d], 0, s1f_r.at[g])
            second(g, origin[d])
    for g in range(2):
        second_forward(g, 0)

    arrival(xref(3, 0), x_r.at[0, 0])
    xsend(3, 0, up, xf_r.at[0])
    xpair(3, 0)
    arrival(xref(1, 1), x_r.at[1, 1])
    xsend(1, 1, down, xf_r.at[1])
    xpair(1, 1)

    for g in range(2):
        arrival(share(g, 2, 0), s1f_r.at[g])
        second(g, 2)
    for j in (3, 1):
        for g in range(2):
            second_forward(g, j)
    arrival(xref(3, 1), x_r.at[0, 1])
    xpair(3, 1)
    arrival(xref(1, 0), x_r.at[1, 0])
    xpair(1, 0)
    for g in range(2):
        second_forward(g, 2)
    arrival(ws.at[0, pl.ds(0, 384), :], s2f_r)
    for g in range(2):
        arrival(ws.at[0, :, pl.ds(g * 384, 384)], loc.at[1 + g])

    arrival(xs.at[pl.ds(0, 3), pl.ds(0, 2)], p_r)

    late = jnp.where(s >= 11, 1, 0)

    def column(q, h):
        return 2 * t + lax.rem(h + q, 2)

    def owner(q, h, c):
        return (lax.rem(q + column(q, h), 4), column(q, h), f, c)

    def att_copies(q):
        my_sequence = q == lax.rem(z + 4 - x, 4)
        found = []
        for h in (1, 0):
            u = column(q, h)
            for c in range(2):
                target = kk.at[s] if c == 0 else vv.at[s, :, pl.ds(0, 128)]
                copy = remote(qkv.at[q, 1 + c], target, a_s, kv_r.at[s], owner(q, h, c))
                elsewhere = jnp.logical_not(my_sequence & (x == u) & (t == c))
                found.append((copy, elsewhere if h == 1 else elsewhere & (s <= 10), h))
        u = column(q, late)
        for c in range(2):
            copy = remote(
                qkv.at[q, 0, pl.ds(c * 128, 128), :], qb.at[s], q_s, q_r, owner(q, late, c)
            )
            found.append((copy, jnp.logical_not(my_sequence & (x == u) & (t == c)), 2))
        return found

    decay = jnp.full((1, 128), decay_rate[f], F32)
    place_rows = lax.broadcasted_iota(jnp.int32, (256, 128), 0).astype(F32)
    key_decay = jnp.exp(-decay * (255.0 - place_rows))

    def project(q, group):
        features = jnp.concatenate([xs[q, lax.rem(f + d, 4)] for d in range(4)], axis=1)
        weights = ws[:, :, group * 384 : group * 384 + 384].reshape(FEATURES, 384)
        total = jnp.dot(features, weights, preferred_element_type=F32).astype(BF16)
        for i in range(3):
            qkv[q, 3 * group + i] = total[:, i * 128 : (i + 1) * 128]

    turn = lax.rem(z + x, 3)

    @pl.loop(0, 4)
    def _(k):
        near = lax.rem(k + turn, 3)
        e = (near + near // 2) * (1 - k // 3) + 2 * (k // 3)
        q = lax.rem(f + e, 4)

        @pl.when(k == 3)
        def _():
            for half in range(2):
                arrival(xref(2, half), xf_r.at[half])
                xpair(2, half)
            arrival(xs.at[0, pl.ds(0, 2)], p2_r)

        project(q, 0)
        for copy, condition, kind in att_copies(q):
            @pl.when(condition if kind else condition & ((k == 0) | (k == 3)))
            def _():
                copy.start()

        kept = (q == lax.rem(z + 4 - x, 4)) & (high == t)

        @pl.when(kept & ((side == 1) | (s <= 10)))
        def _():
            @pl.when(t == 0)
            def _():
                kk[s] = qkv[q, 1]

            @pl.when(t == 1)
            def _():
                vv[s, :, 0:128] = qkv[q, 2]

        @pl.when(kept & (side == late))
        def _():
            qb[s] = qkv[q, 0, pl.ds(pl.multiple_of(t * 128, 128), 128), :]

    @pl.loop(1, 3)
    def _(k):
        near = lax.rem(k + turn, 3)
        for copy, condition, kind in att_copies(lax.rem(f + near + near // 2, 4)):
            if kind == 0:
                @pl.when(condition)
                def _():
                    copy.start()

    @pl.loop(0, 4)
    def _(q):
        project(q, 1)
        decayed = (qkv[q, 4].astype(F32) * key_decay).astype(BF16)
        stat[pl.ds(pl.multiple_of(q * 128, 128), 128), :] = tn_dot(decayed, qkv[q, 5]).astype(BF16)

    def st_copy(i):
        return remote(
            stat.at[pl.ds(pl.multiple_of(i * 32, 32), 32), :], rs.at[s], st_s, st_r,
            (i // 4, lax.rem(i, 4), f, t),
        )

    def pt_copy(i):
        return remote(
            ps.at[i], sin.at[pl.ds(pl.multiple_of(s * 32, 32), 32), :], pt_s, pt_r,
            (i // 4, lax.rem(i, 4), f, t),
        )

    @pl.loop(0, 16)
    def _(i):
        @pl.when(i != s)
        def _():
            st_copy(i).start()

    rs[s] = stat[srow, :]

    decay_square = jnp.broadcast_to(decay[:, 0:1], (256, 256))
    apart = (
        lax.broadcasted_iota(jnp.int32, (256, 256), 0) - lax.broadcasted_iota(jnp.int32, (256, 256), 1)
    ).astype(F32)
    within = jnp.where(apart >= 0, jnp.exp(-decay_square * jnp.maximum(apart, 0.0)), 0.0)

    @pl.loop(0, 4)
    def _(q):
        scores = nt_dot(qkv[q, 3], qkv[q, 4]) * within
        uu[q] = jnp.dot(scores.astype(BF16), qkv[q, 5], preferred_element_type=F32)

    sequence = lax.rem(z + 4 - x, 4)
    head = 4 * high + f
    key_blocks = 11 + 5 * side
    first_block = 11 * side
    kv_buffers = (lambda i: kk.at[i], lambda i: vv.at[i, :, pl.ds(0, 128)])

    def forward_copy(c, i):
        return remote(kv_buffers[c](i), kv_buffers[c](i), f_s, f_r, partner)

    for c in range(2):
        @pl.when(t == c)
        def _():
            @pl.loop(0, key_blocks)
            def _(i):
                @pl.when(jnp.logical_not((i == s) & (high == t)))
                def _():
                    arrival(kv_buffers[c](i), kv_r.at[i])
                forward_copy(c, i).start()

    arrival(gl.at[1 - t], gl_r)

    def one_if(condition):
        return jnp.where(condition, 1, 0)

    def counted(ref, sem, n, *values):
        for k in values:
            @pl.when(n == k)
            def _():
                arrival(ref.at[pl.ds(0, k)], sem)

    queries = 11 - 6 * side
    counted(qb, q_r, queries - one_if((high == t) & (side == late)), 11, 10, 5, 4)
    counted(kk, f_r, key_blocks, 11, 16)

    lam = gl[high, pl.ds(1, 1), :]
    att_gain = gl[high, pl.ds(0, 1), :] * branch_scale
    lane = lax.broadcasted_iota(jnp.int32, (128, 128), 1)
    join_cols = pl.ds(pl.multiple_of(head * 128, 128), 128)

    def att_out(i):
        return remote(
            ob.at[i], join.at[:, join_cols], ja_s, j_r.at[head], (i // 4, lax.rem(i, 4), sequence, t)
        )

    def att_self(i):
        return (i == s) & (sequence == f)

    def attention(first, count, m, height):
        for b in range(count):
            query = qb[first + b].astype(F32) * 0.125
            qs[b * 256 : b * 256 + 128] = jnp.where(lane < 64, query, 0.0).astype(BF16)
            qs[b * 256 + 128 : b * 256 + 256] = jnp.where(lane >= 64, query, 0.0).astype(BF16)
        keys = kk[0 : 2 * m + 2].reshape(512 * m + 512, 128)
        values = vv[0 : 2 * m + 2].reshape(512 * m + 512, 256)
        for b in range(256 * count // height):
            span = slice(b * height, b * height + height)
            scores = nt_dot(qs[span], keys)
            row = lax.broadcasted_iota(jnp.int32, (height, 512), 0) + b * height
            row = lax.rem(row, 128) + 256 * (row // 256) + (128 * t + 256 * (first - 2 * m))
            column = lax.broadcasted_iota(jnp.int32, (height, 512), 1)
            last = jnp.where(column <= row, scores[:, 512 * m :], masked_score)
            scores = jnp.concatenate([scores[:, : 512 * m], last], axis=1) if m else last
            weights = jnp.exp(scores - jnp.max(scores, axis=-1, keepdims=True))
            sums[span] = jnp.dot(weights.astype(BF16), values, preferred_element_type=F32)
        for b in range(count):
            i = first + b
            averaged = sums[b * 256 : b * 256 + 256, 0:128] / sums[b * 256 : b * 256 + 256, 128:256]
            differ = averaged[0:128] - lam * averaged[128:256]
            normed = differ * lax.rsqrt(jnp.mean(differ * differ, axis=-1, keepdims=True) + epsilon)
            result = (normed * att_gain).astype(BF16)
            ob[i] = result

            @pl.when(jnp.logical_not(att_self(i)))
            def _():
                att_out(i).start()

            @pl.when(att_self(i))
            def _():
                join[:, join_cols] = result

    attention(10 + side, 1, 5, 128)

    arrival(rs.at[pl.ds(0, 15)], st_r)

    block_decay = jnp.exp(-decay * 256.0)
    carry = jnp.zeros((32, 128), F32)
    for i in range(16):
        ps[i] = carry.astype(BF16)
        if i < 15:
            carry = carry * block_decay + rs[i].astype(F32)

    @pl.loop(0, 16)
    def _(i):
        @pl.when(i != s)
        def _():
            pt_copy(i).start()

    sin[srow, :] = ps[s]

    @pl.when(side == 0)
    def _():
        for m in range(5):
            attention(2 * m, 2, m, 256)

    @pl.when(side == 1)
    def _():
        for m in (6, 7):
            attention(2 * m, 2, m, 256)

    arrival(sin.at[pl.ds(0, 480), :], pt_r)

    ret_head = 8 + 4 * t + f
    ret_cols = pl.ds(pl.multiple_of(ret_head * 128, 128), 128)
    query_decay = jnp.exp(-decay * (place_rows + 1.0))
    ret_gain = rows[2:3, :]

    def ret_out(q, c):
        return remote(
            rb.at[q, pl.ds(c * 128, 128), :], join.at[:, ret_cols], jr_s, jr_r, (z, x, q, c)
        )

    def ret_self(q, c):
        return (q == f) & (t == c)

    @pl.loop(0, 4)
    def _(q):
        state = sin[pl.ds(pl.multiple_of(q * 128, 128), 128), :]
        u = uu[q] + jnp.dot(qkv[q, 3], state, preferred_element_type=F32) * query_decay
        normed = u * lax.rsqrt(jnp.mean(u * u, axis=-1, keepdims=True) + epsilon)
        rb[q] = (normed * ret_gain).astype(BF16)
        for c in range(2):
            @pl.when(jnp.logical_not(ret_self(q, c)))
            def _():
                ret_out(q, c).start()

            @pl.when(ret_self(q, c))
            def _():
                join[:, ret_cols] = rb[q, c * 128 : (c + 1) * 128, :]

    gl_copy.wait_send()
    ss_copy.wait_send()
    arrival(stage, w1_s)
    arrival(ws.at[pl.ds(0, 3), pl.ds(0, 480), :], w_s)
    arrival(xs.at[pl.ds(0, 3), pl.ds(0, 2)], x_s)
    arrival(xs.at[pl.ds(0, 2)], p_s)
    arrival(rs.at[pl.ds(0, 15)], st_s)
    arrival(ps.at[pl.ds(0, 15)], pt_s)
    kept_kv = one_if((high == t) & ((side == 1) | (s <= 10)))
    counted(kk, a_s, 16 - 8 * late - kept_kv, 16, 15, 8, 7)
    counted(qb, q_s, 8 - one_if((high == t) & (side == late)), 8, 7)
    counted(kk, f_s, key_blocks, 11, 16)

    ow_copy.wait()
    for h in (0, 2, 4, 6):
        for k in (h, h + 1):
            @pl.when(jnp.logical_not((k % 4 == f) & (sequence == f) & (high == k // 4) & (side == late)))
            def _():
                arrival(ob.at[0], j_r.at[k])

        heads = slice(h * 128, h * 128 + 256)
        piece = jnp.dot(join[:, heads], ow[heads, :], preferred_element_type=F32)
        if h == 0:
            summed[...] = piece
        else:
            summed[...] += piece

    arrival(qb.at[pl.ds(0, 7)], jr_r)
    for n in range(4):
        span = slice(n * 512, n * 512 + 512)
        piece = jnp.dot(join[:, 1024:], ow[1024:, span], preferred_element_type=F32)
        rounded[:, span] = (summed[:, span] + piece).astype(BF16)
    out_copy = pltpu.make_async_copy(rounded, out_hbm, loc.at[11])
    out_copy.start()

    counted(ob, ja_s, queries - one_if((sequence == f) & (side == late)), 11, 10, 5, 4)
    arrival(qb.at[pl.ds(0, 7)], jr_s)
    out_copy.wait()


def body(
    tokens, norm_gain, query_weight, key_weight, value_weight, state_query, state_key, state_value,
    map_lambda, diff_gain, decay_rate, state_gain, out_weight,
):
    hbm = pl.BlockSpec(memory_space=pltpu.HBM)
    out = pl.pallas_call(
        kernel,
        out_shape=jax.ShapeDtypeStruct((128, FEATURES), BF16),
        in_specs=[hbm] * 13,
        out_specs=hbm,
        scratch_shapes=[
            pltpu.SMEM((4,), F32),
            pltpu.SMEM((4,), F32),
            pltpu.VMEM((256, 1024), BF16),
            pltpu.VMEM((1, 1024), F32),
            pltpu.VMEM((8, 128), F32),
            pltpu.VMEM((2, 256, 128), F32),
            pltpu.VMEM((2, 8, 128), F32),
            pltpu.VMEM((4, 4, 256, 512), BF16),
            pltpu.VMEM((4, 512, 768), BF16),
            pltpu.VMEM((3, 32, 768), BF16),
            pltpu.VMEM((4, 6, 256, 128), BF16),
            pltpu.VMEM((16, 256, 128), BF16),
            pltpu.VMEM((16, 256, 256), BF16),
            pltpu.VMEM((16, 128, 128), BF16),
            pltpu.VMEM((512, 128), BF16),
            pltpu.VMEM((512, 256), F32),
            pltpu.VMEM((16, 128, 128), BF16),
            pltpu.VMEM((128, FEATURES), BF16),
            pltpu.VMEM((FEATURES, FEATURES), BF16),
            pltpu.VMEM((128, FEATURES), F32),
            pltpu.VMEM((128, FEATURES), BF16),
            pltpu.VMEM((512, 128), BF16),
            pltpu.VMEM((16, 32, 128), BF16),
            pltpu.VMEM((16, 32, 128), BF16),
            pltpu.VMEM((512, 128), BF16),
            pltpu.VMEM((4, 256, 128), F32),
            pltpu.VMEM((4, 256, 128), BF16),
            DMA((12,)), DMA((23,)), DMA((2,)), DMA((2, 2)), DMA((2,)), DMA((2, 4, 2)),
            DMA((2, 2)), DMA((2,)), DMA((16,)), DMA((8,)),
        ],
        compiler_params=pltpu.CompilerParams(
            collective_id=0, has_side_effects=True, vmem_limit_bytes=48 * 1024 * 1024
        ),
        cost_estimate=pl.CostEstimate(flops=40_000_000_000, bytes_accessed=8_000_000, transcendentals=8_000_000),
        name="layer",
    )(
        *(
            pltpu.with_memory_space_constraint(a, pltpu.HBM)
            for a in (
                tokens, norm_gain, diff_gain, state_gain, map_lambda, decay_rate,
                query_weight, key_weight, value_weight, state_query, state_key, state_value, out_weight,
            )
        )
    )
    return out[None]


def solution(mesh):
    torus = Mesh(
        mesh.devices.reshape(4, 4, mesh.shape["fs"], mesh.shape["tp"]), ("sp_0", "sp_1", "fs", "tp")
    )
    return jax.shard_map(
        body,
        mesh=torus,
        in_specs=(
            P("fs", SP, "tp"), P(), P("fs", "tp"), P("fs", "tp"), P("fs", "tp"), P("fs", "tp"), P("fs", "tp"),
            P("fs", "tp"), P("tp"), P("tp"), P("tp"), P("tp"), P(),
        ),
        out_specs=P("fs", SP_TP, None),
        check_vma=False,
    )
```

time: 75.9 us -> 72 us (0.949)
  the two profiles are of different devices: /device:TPU:55 before, /device:TPU:65 now
where the time goes in v4:
time: 72 us; the launch traced here: 71.9 us
  Pallas kernels  71.1 us (99%)
  local copies, waits for them, and re-layouts  0.8 us (1%)
    pallas_call x1, Pallas kernels, body(): pl.pallas_call(kernel, out_shape=jax.ShapeDtypeStruct((128, FEATURES), BF...  71.1 us

profile of v4, /device:TPU:65, one launch (start us, length us, event | category | flops | bytes accessed | tf_op | source)
XLA Modules:
  0.0 71.9 jit_solution(8354494190394198995)
XLA Ops:
  0.0 71.1 %layer.1 = bf16[128,2048]{1,0:T(8,128)(2,1)S(1)} custom-call(bf16[1,256,1024]{2,1,0:T(8,128)(2,1)} %tok_hbm.1, f32[2048]{0:T(1024)} %norm_gain.1, f32[512]{0:T(512)} %diff_gain.1, f32[512]{0:T(512)} %state_gain.1, f32[4]{0:T(128)} %lambda_hbm.1, f32[4]{0:T(128)} %decay_hbm.1, bf16[512,512]{1,0:T(8,128)(2,1)} %wq.1, bf16[512,512]{1,0:T(8,128)(2,1)} %wk.1, ...), custom_call_target="tpu_custom_call" | custom-call | flops 40000000000 | bytes 8000000 | tf_op jit(solution)/shard_map/layer/pallas_call | solution.py:539
  71.1 0.8 %copy.15 = bf16[1,128,2048]{2,1,0:T(8,128)(2,1)} copy(bf16[1,128,2048]{2,1,0:T(8,128)(2,1)S(1)} %bitcast.1) | data formatting | bytes 1048576

commit v5 on v4

--- a/solution.py
+++ b/solution.py
@@ -220,12 +220,12 @@
     for j in (3, 1):
         for g in range(2):
             second_forward(g, j)
+    for g in range(2):
+        second_forward(g, 2)
     arrival(xref(3, 1), x_r.at[0, 1])
     xpair(3, 1)
     arrival(xref(1, 0), x_r.at[1, 0])
     xpair(1, 0)
-    for g in range(2):
-        second_forward(g, 2)
     arrival(ws.at[0, pl.ds(0, 384), :], s2f_r)
     for g in range(2):
         arrival(ws.at[0, :, pl.ds(g * 384, 384)], loc.at[1 + g])
@@ -399,40 +399,56 @@
     def att_self(i):
         return (i == s) & (sequence == f)
 
-    def attention(first, count, m, height):
+    def attention(first, count, m, height, parity):
         for b in range(count):
             query = qb[first + b].astype(F32) * 0.125
-            qs[b * 256 : b * 256 + 128] = jnp.where(lane < 64, query, 0.0).astype(BF16)
-            qs[b * 256 + 128 : b * 256 + 256] = jnp.where(lane >= 64, query, 0.0).astype(BF16)
+            qs[parity, b * 256 : b * 256 + 128] = jnp.where(lane < 64, query, 0.0).astype(BF16)
+            qs[parity, b * 256 + 128 : b * 256 + 256] = jnp.where(lane >= 64, query, 0.0).astype(BF16)
         keys = kk[0 : 2 * m + 2].reshape(512 * m + 512, 128)
         values = vv[0 : 2 * m + 2].reshape(512 * m + 512, 256)
         for b in range(256 * count // height):
             span = slice(b * height, b * height + height)
-            scores = nt_dot(qs[span], keys)
+            scores = nt_dot(qs[parity, span], keys)
             row = lax.broadcasted_iota(jnp.int32, (height, 512), 0) + b * height
             row = lax.rem(row, 128) + 256 * (row // 256) + (128 * t + 256 * (first - 2 * m))
             column = lax.broadcasted_iota(jnp.int32, (height, 512), 1)
             last = jnp.where(column <= row, scores[:, 512 * m :], masked_score)
             scores = jnp.concatenate([scores[:, : 512 * m], last], axis=1) if m else last
             weights = jnp.exp(scores - jnp.max(scores, axis=-1, keepdims=True))
-            sums[span] = jnp.dot(weights.astype(BF16), values, preferred_element_type=F32)
+            sums[parity, span] = jnp.dot(weights.astype(BF16), values, preferred_element_type=F32)
+
+    def finish(first, count, parity):
         for b in range(count):
-            i = first + b
-            averaged = sums[b * 256 : b * 256 + 256, 0:128] / sums[b * 256 : b * 256 + 256, 128:256]
+            found = sums[parity, b * 256 : b * 256 + 256, :]
+            averaged = found[:, 0:128] / found[:, 128:256]
             differ = averaged[0:128] - lam * averaged[128:256]
             normed = differ * lax.rsqrt(jnp.mean(differ * differ, axis=-1, keepdims=True) + epsilon)
-            result = (normed * att_gain).astype(BF16)
-            ob[i] = result
-
+            ob[first + b] = (normed * att_gain).astype(BF16)
+
+    def deliver(first, count):
+        for i in (first + b for b in range(count)):
             @pl.when(jnp.logical_not(att_self(i)))
             def _():
                 att_out(i).start()
 
             @pl.when(att_self(i))
             def _():
-                join[:, join_cols] = result
-
-    attention(10 + side, 1, 5, 128)
+                join[:, join_cols] = ob[i]
+
+    def attention_pairs(pairs):
+        before = None
+        for n, m in enumerate(pairs):
+            attention(2 * m, 2, m, 256, n % 2)
+            if before is not None:
+                finish(2 * before, 2, (n + 1) % 2)
+                deliver(2 * before, 2)
+            before = m
+        finish(2 * before, 2, (len(pairs) + 1) % 2)
+        deliver(2 * before, 2)
+
+    attention(10 + side, 1, 5, 128, 0)
+    finish(10 + side, 1, 0)
+    deliver(10 + side, 1)
 
     arrival(rs.at[pl.ds(0, 15)], st_r)
 
@@ -453,13 +469,11 @@
 
     @pl.when(side == 0)
     def _():
-        for m in range(5):
-            attention(2 * m, 2, m, 256)
+        attention_pairs(range(5))
 
     @pl.when(side == 1)
     def _():
-        for m in (6, 7):
-            attention(2 * m, 2, m, 256)
+        attention_pairs((6, 7))
 
     arrival(sin.at[pl.ds(0, 480), :], pt_r)
 
@@ -556,8 +570,8 @@
             pltpu.VMEM((16, 256, 128), BF16),
             pltpu.VMEM((16, 256, 256), BF16),
             pltpu.VMEM((16, 128, 128), BF16),
-            pltpu.VMEM((512, 128), BF16),
-            pltpu.VMEM((512, 256), F32),
+            pltpu.VMEM((2, 512, 128), BF16),
+            pltpu.VMEM((2, 512, 256), F32),
             pltpu.VMEM((16, 128, 128), BF16),
             pltpu.VMEM((128, FEATURES), BF16),
             pltpu.VMEM((FEATURES, FEATURES), BF16),

time: 72 us -> 71.9 us (level)
  no operation moved by 1% of the time
where the time goes in v5:
time: 71.9 us; the launch traced here: 71.8 us
  Pallas kernels  71 us (99%)
  local copies, waits for them, and re-layouts  0.8 us (1%)
    pallas_call x1, Pallas kernels, body(): pl.pallas_call(kernel, out_shape=jax.ShapeDtypeStruct((128, FEATURES), BF...  71 us

profile of v5, /device:TPU:65, one launch (start us, length us, event | category | flops | bytes accessed | tf_op | source)
XLA Modules:
  0.0 71.8 jit_solution(1241923729028712756)
XLA Ops:
  0.0 71.0 %layer.1 = bf16[128,2048]{1,0:T(8,128)(2,1)S(1)} custom-call(bf16[1,256,1024]{2,1,0:T(8,128)(2,1)} %tok_hbm.1, f32[2048]{0:T(1024)} %norm_gain.1, f32[512]{0:T(512)} %diff_gain.1, f32[512]{0:T(512)} %state_gain.1, f32[4]{0:T(128)} %lambda_hbm.1, f32[4]{0:T(128)} %decay_hbm.1, bf16[512,512]{1,0:T(8,128)(2,1)} %wq.1, bf16[512,512]{1,0:T(8,128)(2,1)} %wk.1, ...), custom_call_target="tpu_custom_call" | custom-call | flops 40000000000 | bytes 8000000 | tf_op jit(solution)/shard_map/layer/pallas_call | solution.py:553
  71.0 0.8 %copy.15 = bf16[1,128,2048]{2,1,0:T(8,128)(2,1)} copy(bf16[1,128,2048]{2,1,0:T(8,128)(2,1)S(1)} %bitcast.1) | data formatting | bytes 1048576

commit v6 on v5

--- a/solution.py
+++ b/solution.py
@@ -286,7 +286,7 @@
 
         project(q, 0)
         for copy, condition, kind in att_copies(q):
-            @pl.when(condition if kind else condition & ((k == 0) | (k == 3)))
+            @pl.when(condition)
             def _():
                 copy.start()
 
@@ -305,15 +305,6 @@
         @pl.when(kept & (side == late))
         def _():
             qb[s] = qkv[q, 0, pl.ds(pl.multiple_of(t * 128, 128), 128), :]
-
-    @pl.loop(1, 3)
-    def _(k):
-        near = lax.rem(k + turn, 3)
-        for copy, condition, kind in att_copies(lax.rem(f + near + near // 2, 4)):
-            if kind == 0:
-                @pl.when(condition)
-                def _():
-                    copy.start()
 
     @pl.loop(0, 4)
     def _(q):

time: 71.9 us -> 70.9 us (0.986)
  Pallas kernels: 71 us -> 70 us
    pallas_call x1, Pallas kernels: 71 us -> 70 us  [body(): pl.pallas_call(kernel, out_shape=jax.ShapeDtypeStruct((128, FEATURES), BF...]
where the time goes in v6:
time: 70.9 us; the launch traced here: 70.8 us
  Pallas kernels  70 us (99%)
  local copies, waits for them, and re-layouts  0.8 us (1%)
    pallas_call x1, Pallas kernels, body(): pl.pallas_call(kernel, out_shape=jax.ShapeDtypeStruct((128, FEATURES), BF...  70 us

profile of v6, /device:TPU:65, one launch (start us, length us, event | category | flops | bytes accessed | tf_op | source)
XLA Modules:
  0.0 70.8 jit_solution(10316565776127161658)
XLA Ops:
  0.0 70.0 %layer.1 = bf16[128,2048]{1,0:T(8,128)(2,1)S(1)} custom-call(bf16[1,256,1024]{2,1,0:T(8,128)(2,1)} %tok_hbm.1, f32[2048]{0:T(1024)} %norm_gain.1, f32[512]{0:T(512)} %diff_gain.1, f32[512]{0:T(512)} %state_gain.1, f32[4]{0:T(128)} %lambda_hbm.1, f32[4]{0:T(128)} %decay_hbm.1, bf16[512,512]{1,0:T(8,128)(2,1)} %wq.1, bf16[512,512]{1,0:T(8,128)(2,1)} %wk.1, ...), custom_call_target="tpu_custom_call" | custom-call | flops 40000000000 | bytes 8000000 | tf_op jit(solution)/shard_map/layer/pallas_call | solution.py:544
  70.0 0.8 %copy.15 = bf16[1,128,2048]{2,1,0:T(8,128)(2,1)} copy(bf16[1,128,2048]{2,1,0:T(8,128)(2,1)S(1)} %bitcast.1) | data formatting | bytes 1048576

commit v7 on v6

--- a/solution.py
+++ b/solution.py
@@ -269,7 +269,7 @@
         for i in range(3):
             qkv[q, 3 * group + i] = total[:, i * 128 : (i + 1) * 128]
 
-    turn = lax.rem(z + x, 3)
+    turn = lax.rem(z + 2 * x, 3)
 
     @pl.loop(0, 4)
     def _(k):

time: 70.9 us -> 70.1 us (0.989)
  Pallas kernels: 70 us -> 69.2 us
    pallas_call x1, Pallas kernels: 70 us -> 69.2 us  [body(): pl.pallas_call(kernel, out_shape=jax.ShapeDtypeStruct((128, FEATURES), BF...]
where the time goes in v7:
time: 70.1 us; the launch traced here: 70 us
  Pallas kernels  69.2 us (99%)
  local copies, waits for them, and re-layouts  0.8 us (1%)
    pallas_call x1, Pallas kernels, body(): pl.pallas_call(kernel, out_shape=jax.ShapeDtypeStruct((128, FEATURES), BF...  69.2 us

profile of v7, /device:TPU:65, one launch (start us, length us, event | category | flops | bytes accessed | tf_op | source)
XLA Modules:
  0.0 70.0 jit_solution(15961952185784369101)
XLA Ops:
  0.0 69.2 %layer.1 = bf16[128,2048]{1,0:T(8,128)(2,1)S(1)} custom-call(bf16[1,256,1024]{2,1,0:T(8,128)(2,1)} %tok_hbm.1, f32[2048]{0:T(1024)} %norm_gain.1, f32[512]{0:T(512)} %diff_gain.1, f32[512]{0:T(512)} %state_gain.1, f32[4]{0:T(128)} %lambda_hbm.1, f32[4]{0:T(128)} %decay_hbm.1, bf16[512,512]{1,0:T(8,128)(2,1)} %wq.1, bf16[512,512]{1,0:T(8,128)(2,1)} %wk.1, ...), custom_call_target="tpu_custom_call" | custom-call | flops 40000000000 | bytes 8000000 | tf_op jit(solution)/shard_map/layer/pallas_call | solution.py:544
  69.2 0.8 %copy.15 = bf16[1,128,2048]{2,1,0:T(8,128)(2,1)} copy(bf16[1,128,2048]{2,1,0:T(8,128)(2,1)S(1)} %bitcast.1) | data formatting | bytes 1048576

commit v8 on v7

--- a/solution.py
+++ b/solution.py
@@ -38,8 +38,8 @@
 
 
 def kernel(
-    tok_hbm, norm_gain, diff_gain, state_gain, lambda_hbm, decay_hbm, wq, wk, wv, sq, sk, sv, ow_hbm, out_hbm,
-    map_lambda, decay_rate, tok, gain, rows, ss, gl, xs, ws, stage, qkv, kk, vv, qb, qs, sums, ob, join, ow, summed, rounded, stat, rs, ps, sin, uu, rb,
+    tok_hbm, norm_gain, diff_gain, state_gain, lambda_hbm, decay_hbm, wq, wk, wv, sq, sk, sv, ow_hbm, out,
+    map_lambda, decay_rate, tok, gain, rows, ss, gl, xs, ws, stage, qkv, kk, vv, qb, qs, sums, ob, join, ow, summed, stat, rs, ps, sin, uu, rb,
     loc, once, w1_r, s1_r, s1f_r, s2_r, x_r, xf_r, kv_r, j_r,
 ):
     (
@@ -527,13 +527,9 @@
     for n in range(4):
         span = slice(n * 512, n * 512 + 512)
         piece = jnp.dot(join[:, 1024:], ow[1024:, span], preferred_element_type=F32)
-        rounded[:, span] = (summed[:, span] + piece).astype(BF16)
-    out_copy = pltpu.make_async_copy(rounded, out_hbm, loc.at[11])
-    out_copy.start()
-
+        out[:, span] = (summed[:, span] + piece).astype(BF16)
     counted(ob, ja_s, queries - one_if((sequence == f) & (side == late)), 11, 10, 5, 4)
     arrival(qb.at[pl.ds(0, 7)], jr_s)
-    out_copy.wait()
 
 
 def body(
@@ -545,7 +541,7 @@
         kernel,
         out_shape=jax.ShapeDtypeStruct((128, FEATURES), BF16),
         in_specs=[hbm] * 13,
-        out_specs=hbm,
+        out_specs=pl.BlockSpec(memory_space=pltpu.VMEM),
         scratch_shapes=[
             pltpu.SMEM((4,), F32),
             pltpu.SMEM((4,), F32),
@@ -567,14 +563,13 @@
             pltpu.VMEM((128, FEATURES), BF16),
             pltpu.VMEM((FEATURES, FEATURES), BF16),
             pltpu.VMEM((128, FEATURES), F32),
-            pltpu.VMEM((128, FEATURES), BF16),
             pltpu.VMEM((512, 128), BF16),
             pltpu.VMEM((16, 32, 128), BF16),
             pltpu.VMEM((16, 32, 128), BF16),
             pltpu.VMEM((512, 128), BF16),
             pltpu.VMEM((4, 256, 128), F32),
             pltpu.VMEM((4, 256, 128), BF16),
-            DMA((12,)), DMA((23,)), DMA((2,)), DMA((2, 2)), DMA((2,)), DMA((2, 4, 2)),
+            DMA((11,)), DMA((23,)), DMA((2,)), DMA((2, 2)), DMA((2,)), DMA((2, 4, 2)),
             DMA((2, 2)), DMA((2,)), DMA((16,)), DMA((8,)),
         ],
         compiler_params=pltpu.CompilerParams(

time: 70.1 us -> 70 us (level)
  no operation moved by 1% of the time
where the time goes in v8:
time: 70 us; the launch traced here: 69.9 us
  Pallas kernels  69.1 us (99%)
  local copies, waits for them, and re-layouts  0.8 us (1%)
    pallas_call x1, Pallas kernels, body(): pl.pallas_call(kernel, out_shape=jax.ShapeDtypeStruct((128, FEATURES), BF...  69.1 us

profile of v8, /device:TPU:65, one launch (start us, length us, event | category | flops | bytes accessed | tf_op | source)
XLA Modules:
  0.0 69.9 jit_solution(5380089809553027743)
XLA Ops:
  0.0 69.1 %layer.1 = bf16[128,2048]{1,0:T(8,128)(2,1)S(1)} custom-call(bf16[1,256,1024]{2,1,0:T(8,128)(2,1)} %tok_hbm.1, f32[2048]{0:T(1024)} %norm_gain.1, f32[512]{0:T(512)} %diff_gain.1, f32[512]{0:T(512)} %state_gain.1, f32[4]{0:T(128)} %lambda_hbm.1, f32[4]{0:T(128)} %decay_hbm.1, bf16[512,512]{1,0:T(8,128)(2,1)} %wq.1, bf16[512,512]{1,0:T(8,128)(2,1)} %wk.1, ...), custom_call_target="tpu_custom_call" | custom-call | flops 40000000000 | bytes 8000000 | tf_op jit(solution)/shard_map/layer/pallas_call | solution.py:540
  69.1 0.8 %copy.15 = bf16[1,128,2048]{2,1,0:T(8,128)(2,1)} copy(bf16[1,128,2048]{2,1,0:T(8,128)(2,1)S(1)} %bitcast.1) | data formatting | bytes 1048576
